TPU v7x, 1024 devices: a whole 4x8x16 slice. The times are simulated.
1024 devices in a mesh: gr: 2 (over z_hi), sp: 64 (over z_lo, y), tp: 8 (over x, core).
Axes of the slice: x: 4, y: 8, z: 16 (z_hi: 2, z_lo: 8; z = z_hi * 8 + z_lo), core: 2. Of those that a mesh axis runs over, the one named last changes fastest.
Arguments:
- tokens: bfloat16 [64, 8192, 2048], P(('gr', 'tp'), 'sp'), may hold values from -6 to 6
- kv_weight: bfloat16 [2048, 1024], replicated, may hold values from -0.125 to 0.125
- queries: bfloat16 [64, 1536], P(('gr', 'tp')), may hold values from -6 to 6
- score_offset: float32 [24], replicated, may hold values from -10.5 to -3.5
Outputs:
- cache: bfloat16 [16, 64, 8192, 64], P(('gr', 'tp'), 'sp')
- read: bfloat16 [64, 1536], P(('gr', 'tp'))
All inputs are finite; a program needn't handle non-finite values.
Results may differ from a plain program's by a relative error of at most 0.0085.
Values may be sent and summed in bfloat16 or wider, within the bound.
No kernel may reach another device: no remote copies, remote signals or barrier semaphores. Data moves between devices by JAX's collectives and lax.ppermute only.
A program may use at most 32 MiB of HBM per device.

v0:
```python
import jax
import jax.numpy as jnp
from jax import lax
from jax.sharding import Mesh
from jax.sharding import PartitionSpec as P

KVH = 8
HD = 64
SP = ("sp_0", "sp_1")


def by_axis(shard, axes):
    for axis in axes:
        shard = lax.psum(shard, axis)
    return shard


def shifted(block, axis, distance):
    devices = range(lax.axis_size(axis))
    route = [(i - distance, i) for i in devices if i - distance in devices]
    return lax.ppermute(block, axis, route)


def finish(contribution):
    return by_axis(contribution, SP).astype(jnp.bfloat16)


def local(tokens, kv_weight, queries, score_offset):
    seq_count, pos_rows, model_width = tokens.shape
    features = kv_weight.shape[1]
    slot_count = lax.axis_size(SP)
    blocks = slot_count // seq_count
    block_width = features // blocks
    half_blocks = blocks // 2
    heads = score_offset.shape[0]
    group_size = heads // KVH
    per_block = block_width // HD
    projected = jnp.einsum(
        "spd,dcw->scpw",
        tokens,
        kv_weight.reshape(model_width, blocks, block_width),
        preferred_element_type=jnp.float32,
    ).astype(jnp.bfloat16)
    received = lax.all_to_all(
        projected.reshape(slot_count, pos_rows, block_width),
        SP,
        split_axis=0,
        concat_axis=1,
        tiled=True,
    )
    length = received.shape[1]
    cache = received.reshape(1, 1, length, block_width)
    position = lax.axis_index(SP)
    seq_slot = position // blocks
    head_block = position % blocks
    pair_block = head_block % half_blocks
    span = per_block * group_size
    own_rows = received.reshape(length, per_block, HD)
    query_row = lax.dynamic_slice(
        queries, (seq_slot, pair_block * span * HD), (1, span * HD)
    ).reshape(per_block, group_size, HD)
    offsets = lax.dynamic_slice_in_dim(score_offset, pair_block * span, span).reshape(
        per_block, group_size
    )
    logits = jnp.einsum("vgd,pvd->vgp", query_row, own_rows, preferred_element_type=jnp.float32)
    logits = logits * HD ** (-0.5) + offsets[:, :, None]
    keep_log = jax.nn.log_sigmoid(-logits)
    between = lax.cumsum(keep_log, axis=2, reverse=True) - keep_log
    weights = jnp.exp(jax.nn.log_sigmoid(logits) + between)
    arrived = shifted(weights, SP, half_blocks)
    weighted = jnp.einsum("vgp,pvd->vgd", arrived, own_rows.astype(jnp.float32))
    is_value = (head_block >= half_blocks).astype(jnp.float32)
    contribution = lax.dynamic_update_slice(
        jnp.zeros((seq_count, heads * HD), jnp.float32),
        (weighted * is_value).reshape(1, span * HD),
        (seq_slot, pair_block * span * HD),
    )
    return (cache, finish(contribution))


def solution(mesh):
    torus = Mesh(
        mesh.devices.reshape(mesh.shape["gr"], 8, 8, mesh.shape["tp"]), ("gr", "sp_0", "sp_1", "tp")
    )
    return jax.shard_map(
        local,
        mesh=torus,
        in_specs=(P(("gr", "tp"), SP, None), P(), P(("gr", "tp"), None), P()),
        out_specs=(P(("gr", "tp"), SP, None, None), P(("gr", "tp"), None)),
        check_vma=False,
    )
```

profile of v0, /device:TPU:6, one launch (start us, length us, event | category | flops | bytes accessed | tf_op | source)
XLA Modules:
  0.0 180.0 jit_solution(5396815822232727855)
XLA Ops:
  0.6 6.7 %copy.10 = bf16[2048,1024]{0,1:T(8,128)(2,1)} copy(bf16[2048,1024]{1,0:T(8,128)(2,1)} %param.5) | data formatting | bytes 8388608 | tf_op args[1]
  7.3 4.5 %fusion.6 = bf16[4,16,128,64]{2,3,0,1:T(8,128)(2,1)S(1)} fusion(bf16[2048,16,64,1]{0,2,3,1:T(8,128)(2,1)} %bitcast.57, bf16[4,128,2048]{2,1,0:T(8,128)(2,1)S(1)} %copy-done), kind=kOutput, calls=%fused_computation.5 | convolution fusion | flops 2148007936 | bytes 7340032 | tf_op jit(solution)/shard_map/spd,dcw->scpw/dot_general | solution.py:38
  11.9 1.1 copy.11
  12.9 22.0 %all-to-all-start = ((bf16[64,128,64]{1,2,0:T(8,128)(2,1)}), bf16[64,128,64]{1,2,0:T(8,128)(2,1)S(1)}, u32[]{:S(2)}, u32[]{:S(2)}) async-start(bf16[64,128,64]{1,2,0:T(8,128)(2,1)} %bitcast.58), calls=%async_computation | async-start | bytes 2097152 | tf_op jit(solution)/shard_map/all_to_all | solution.py:44
  35.0 0.8 dynamic-slice_reduce_fusion
  35.7 0.1 reshape.91
  35.8 0.1 dynamic_slice.7
  35.9 51.2 %all-to-all-done = bf16[64,128,64]{1,2,0:T(8,128)(2,1)S(1)} async-done(((bf16[64,128,64]{1,2,0:T(8,128)(2,1)}), bf16[64,128,64]{1,2,0:T(8,128)(2,1)S(1)}, u32[]{:S(2)}, u32[]{:S(2)}) %all-to-all-start) | async-done | bytes 1048608 | tf_op jit(solution)/shard_map/all_to_all | solution.py:44
  87.1 0.2 fusion
  87.4 0.2 fusion.20
  87.6 3.8 %reduce-window.6 = f32[1,3,64,128]{3,2,1,0:T(8,128)S(1)} reduce-window(f32[1,3,64,128]{3,2,1,0:T(8,128)S(1)} %copy.31, f32[]{:T(128)} %constant.49.clone.1), window={size=1x1x1x128 pad=0_0x0_0x0_0x0_127}, to_apply=%region_0.1 | reduce-window | flops 3121152 | bytes 196612 | tf_op jit(solution)/shard_map/reduce-window
  91.3 0.1 slice_reduce_fusion
  91.4 0.5 reduce-window.9
  91.9 0.1 slice_bitcast_fusion
  92.0 0.1 broadcast_bitcast_fusion
  92.1 0.4 fusion.16
  92.5 1.3 collective-permute-start
  93.8 1.7 copy.12
  95.5 2.3 %reshape.90 = bf16[1,1,8192,64]{2,3,1,0:T(8,128)(2,1)} reshape(bf16[64,128,64]{1,0,2:T(8,128)(2,1)} %copy.12) | data formatting | bytes 2097152 | tf_op jit(solution)/shard_map/reshape | solution.py:52
  97.8 0.4 convolution_multiply_fusion.1
  98.1 0.1 reshape.99
  98.2 0.2 dynamic_update_slice.3
  98.4 53.3 %psum.14 = f32[4,1536]{1,0:T(4,128)S(1)} all-reduce(f32[4,1536]{1,0:T(4,128)S(1)} %dynamic_update_slice.3), channel_id=1, replica_groups=mesh['gr'=2,'sp_0'=8,'sp_1'=8,'tp'=8] {'sp_0'}, use_global_device_ids=true, to_apply=%region_2.3 | all-reduce | flops 6144 | bytes 49152 | tf_op jit(solution)/shard_map/psum | solution.py:14
  151.7 28.2 %psum.15 = bf16[4,1536]{1,0:T(4,128)(2,1)} all-reduce(f32[4,1536]{1,0:T(4,128)S(1)} %psum.14), channel_id=1, replica_groups=mesh['gr'=2,'sp_0'=8,'sp_1'=8,'tp'=8] {'sp_1'}, use_global_device_ids=true, to_apply=%region_3.4 | all-reduce | flops 6144 | bytes 36864 | tf_op jit(solution)/shard_map/psum | solution.py:14
  (7 shorter events, 0.0 us)
Async XLA Ops:
  0.6 6.7 %copy-start = (bf16[4,128,2048]{2,1,0:T(8,128)(2,1)S(1)}, bf16[4,128,2048]{2,1,0:T(8,128)(2,1)}, u32[]{:S(2)}) copy-start(bf16[4,128,2048]{2,1,0:T(8,128)(2,1)} %param.4) | copy-start | bytes 6291460
  11.9 24.0 %copy-start.1 = (f32[24]{0:T(128)S(1)}, f32[24]{0:T(128)}, u32[]{:S(2)}) copy-start(f32[24]{0:T(128)} %param.7) | copy-start | bytes 292
  12.9 74.2 %all-to-all-start = ((bf16[64,128,64]{1,2,0:T(8,128)(2,1)}), bf16[64,128,64]{1,2,0:T(8,128)(2,1)S(1)}, u32[]{:S(2)}, u32[]{:S(2)}) async-start(bf16[64,128,64]{1,2,0:T(8,128)(2,1)} %bitcast.58), calls=%async_computation | async-start | bytes 2097152 | tf_op jit(solution)/shard_map/all_to_all | solution.py:44
  92.5 5.3 %collective-permute-start = (bf16[1,3,8192]{2,1,0:T(4,128)(2,1)S(1)}, bf16[1,3,8192]{2,1,0:T(4,128)(2,1)S(1)}, u32[]{:S(2)}, u32[]{:S(2)}) collective-permute-start(bf16[1,3,8192]{2,1,0:T(4,128)(2,1)S(1)} %fusion.16), channel_id=1, source_target_pairs={{0,64},{8,72},{16,80},{24,88},{32,96},{40,104},{48,112},{56,120},{... | collective-permute-start | bytes 147464 | tf_op jit(solution)/shard_map/ppermute | solution.py:21
where the time goes:
time: 180 us
  blocking collectives  81.5 us (45%)
  waiting for transfers between devices  51.2 us (28%)
  starting transfers between devices  23.3 us (13%)
  local copies, waits for them, and re-layouts  13.2 us (7%)
  matrix products  5.16 us (3%)
  other arithmetic  4.79 us (3%)
    psum x2, blocking collectives, by_axis(): shard = lax.psum(shard, axis)  81.5 us
    all_to_all x1, waiting for transfers between devices, local(): lax.all_to_all(projected.reshape(slot_count, pos_rows, block_width), SP,...  51.2 us
    all_to_all x1, starting transfers between devices, local(): lax.all_to_all(projected.reshape(slot_count, pos_rows, block_width), SP,...  22 us
    unnamed x7, local copies, waits for them, and re-layouts  6.76 us
    dot_general x1, matrix products, local(): jnp.einsum('spd,dcw->scpw', tokens, kv_weight.reshape(model_width, blocks...  4.54 us
    another operation x2, other arithmetic  4.23 us
  transfers between devices with their start and end apart: 2, of which 1 were waited for; matrix products, arithmetic and copies ran while one was open for 3% of the time, Pallas kernels for 0%

commit v1 on v0

v1 whole, which is shorter than its diff:
```python
import functools

import jax
import jax.numpy as jnp
from jax import lax
from jax.experimental import pallas as pl
from jax.experimental.pallas import tpu as pltpu
from jax.sharding import Mesh
from jax.sharding import PartitionSpec as P


KVH = 8
HD = 64
LANES = 128
SLOT = 32
SP = ("sp_0", "sp_1")
VMEM = pltpu.VMEM


def small(mebibytes):
    return pltpu.CompilerParams(vmem_limit_bytes=mebibytes * 1024 * 1024)


def project_kernel(x_ref, w_ref, out_ref):
    seqs, rows, depth = x_ref.shape
    acc = jnp.dot(
        x_ref[...].reshape(seqs * rows, depth), w_ref[...], preferred_element_type=jnp.float32
    )
    for q in range(seqs):
        turned = acc[q * rows : (q + 1) * rows].T
        out_ref[q] = turned.reshape(out_ref.shape[1:]).astype(out_ref.dtype)


def project(tokens, kv_weight, blocks):
    seqs, rows, depth = tokens.shape
    features = kv_weight.shape[1]
    width = features // blocks
    step = 256
    return pl.pallas_call(
        project_kernel,
        grid=(features // step,),
        in_specs=[
            pl.BlockSpec((seqs, rows, depth), lambda j: (0, 0, 0)),
            pl.BlockSpec((depth, step), lambda j: (0, j)),
        ],
        out_specs=pl.BlockSpec((seqs, step // width, width, rows), lambda j: (0, j, 0, 0)),
        out_shape=jax.ShapeDtypeStruct((seqs, blocks, width, rows), jnp.bfloat16),
        name="project",
    )(tokens, kv_weight)


def stick_kernel(heads, kv_ref, q_ref, off_ref, out_ref):
    seqs = kv_ref.shape[0]
    group = heads // KVH
    f32 = jnp.float32
    row_head = lax.broadcasted_iota(jnp.int32, (SLOT, LANES), 0) // group
    logits = []
    for s in range(seqs):
        queries = q_ref[s * SLOT : (s + 1) * SLOT]
        total = jnp.zeros((SLOT, LANES), f32)
        for n in range(KVH):
            part = jnp.dot(queries, kv_ref[s, n], preferred_element_type=f32)
            total = jnp.where(row_head == n, part, total)
        logits.append(total)
    logit = jnp.concatenate(logits, axis=0) * HD ** (-0.5) + off_ref[...]
    soft = jnp.log1p(jnp.exp(-jnp.abs(logit)))
    log_take = jnp.minimum(logit, 0.0) - soft
    keep = jnp.minimum(-logit, 0.0) - soft
    r = lax.broadcasted_iota(jnp.int32, (LANES, LANES), 0)
    c = lax.broadcasted_iota(jnp.int32, (LANES, LANES), 1)
    later = (r > c).astype(f32)
    between = jnp.dot(keep, later, preferred_element_type=f32, precision=lax.Precision.HIGHEST)
    weight = jnp.exp(log_take + between)
    high = weight.astype(jnp.bfloat16)
    low = (weight - high.astype(f32)).astype(jnp.bfloat16)
    lane = lax.broadcasted_iota(jnp.int32, (HD, LANES), 1)
    lane_seq, lane_head = lane // SLOT, (lane % SLOT) // group
    dims = (((1,), (1,)), ((), ()))
    total = jnp.zeros((HD, LANES), f32)
    for s in range(seqs):
        values = kv_ref[s, KVH:].reshape(KVH * HD, LANES)
        product = lax.dot_general(values, high, dims, preferred_element_type=f32)
        product += lax.dot_general(values, low, dims, preferred_element_type=f32)
        for n in range(KVH):
            mine = (lane_seq == s) & (lane_head == n)
            total = jnp.where(mine, product[n * HD : (n + 1) * HD], total)
    out_ref[:HD] = total
    out_ref[HD:] = lax.dot_general(
        jnp.ones((8, LANES), f32), keep, dims, preferred_element_type=f32,
        precision=lax.Precision.HIGHEST,
    )


def stick(projected, queries, score_offset):
    seqs = queries.shape[0]
    heads = score_offset.shape[0]
    spare = SLOT - heads
    rows = jnp.pad(queries.reshape(seqs, heads, HD), ((0, 0), (0, spare), (0, 0)))
    offsets = jnp.tile(jnp.pad(score_offset, (0, spare)), seqs)[:, None]
    return pl.pallas_call(
        functools.partial(stick_kernel, heads),
        in_specs=[pl.BlockSpec(memory_space=VMEM)] * 3,
        out_specs=pl.BlockSpec(memory_space=VMEM),
        out_shape=jax.ShapeDtypeStruct((HD + 8, LANES), jnp.float32),
        compiler_params=small(4),
        name="stick",
    )(projected, rows.reshape(seqs * SLOT, HD), offsets)


def partner(block, axis, distance):
    return lax.ppermute(block, axis, [(i, i ^ distance) for i in range(lax.axis_size(axis))])


def pack(state):
    total = state[HD:]
    high = total.astype(jnp.bfloat16).astype(jnp.float32)
    middle = (total - high).astype(jnp.bfloat16).astype(jnp.float32)
    row = lax.broadcasted_iota(jnp.int32, total.shape, 0)
    parts = jnp.where(row == 0, high, jnp.where(row == 1, middle, total - high - middle))
    return jnp.concatenate([state[:HD], parts], axis=0).astype(jnp.bfloat16)


def join_kernel(axis, distance, own_ref, other_ref, out_ref):
    own_first = (lax.axis_index(axis) & distance) == 0
    own, other = own_ref[...], other_ref[...]
    first = jnp.where(own_first, own, other)
    last = jnp.where(own_first, other, own)
    values = first[:HD] * jnp.exp(last[HD : HD + 1]) + last[:HD]
    state = jnp.concatenate([values, first[HD:] + last[HD:]], axis=0)
    out_ref[...] = pack(state) if out_ref.dtype == jnp.bfloat16 else state


def join(own, other, axis, distance, dtype):
    return pl.pallas_call(
        functools.partial(join_kernel, axis, distance),
        in_specs=[pl.BlockSpec(memory_space=VMEM)] * 2,
        out_specs=pl.BlockSpec(memory_space=VMEM),
        out_shape=jax.ShapeDtypeStruct(own.shape, dtype),
        compiler_params=small(1),
        name="join",
    )(own, other)


def finish_kernel(heads, own_ref, other_ref, out_ref, turned, wide):
    seqs = out_ref.shape[0]
    place = lax.axis_index("sp_0")
    total = jnp.zeros((HD, LANES), jnp.float32)
    after = jnp.zeros((1, LANES), jnp.float32)
    half = own_ref.shape[0]
    for z in reversed(range(2 * half)):
        at = place ^ z
        state = jnp.where(at % 2 == 0, own_ref[at // 2].astype(jnp.float32), other_ref[at // 2].astype(jnp.float32))
        total += state[:HD] * jnp.exp(after)
        after += state[HD : HD + 1] + state[HD + 1 : HD + 2] + state[HD + 2 : HD + 3]
    turned[...] = jnp.concatenate([total, total], axis=0).T
    for h in range(heads):
        wide[:, h * HD : (h + 1) * HD] = turned[pl.ds(h, seqs, stride=SLOT), :][:, :HD]
    out_ref[...] = wide[...].astype(out_ref.dtype)


def finish(own, other, seqs, heads):
    return pl.pallas_call(
        functools.partial(finish_kernel, heads),
        in_specs=[pl.BlockSpec(memory_space=VMEM)] * 2,
        out_specs=pl.BlockSpec(memory_space=VMEM),
        out_shape=jax.ShapeDtypeStruct((seqs, heads * HD), jnp.bfloat16),
        scratch_shapes=[
            pltpu.VMEM((LANES, LANES), jnp.float32),
            pltpu.VMEM((seqs, heads * HD), jnp.float32),
        ],
        compiler_params=small(1),
        name="finish",
    )(own, other)


def lay_kernel(in_ref, out_ref, sem):
    sources, _, rows = in_ref.shape
    for i in range(sources):
        pltpu.make_async_copy(in_ref.at[i], out_ref.at[:, pl.ds(i * rows, rows)], sem).start()
    pltpu.make_async_copy(out_ref, out_ref, sem).wait()


def lay(received):
    sources, width, rows = received.shape
    return pl.pallas_call(
        lay_kernel,
        in_specs=[pl.BlockSpec(memory_space=pl.ANY)],
        out_specs=pl.BlockSpec(memory_space=pl.ANY),
        out_shape=jax.ShapeDtypeStruct((width, sources * rows), received.dtype),
        scratch_shapes=[pltpu.SemaphoreType.DMA],
        compiler_params=small(1),
        name="lay",
    )(received)


def local(tokens, kv_weight, queries, score_offset):
    seqs, rows, _ = tokens.shape
    features = kv_weight.shape[1]
    slots = lax.axis_size(SP)
    blocks = slots // seqs
    width = features // blocks
    heads = score_offset.shape[0]

    projected = project(tokens, kv_weight, blocks)
    received = lax.all_to_all(
        projected.reshape(slots, width, rows), SP, split_axis=0, concat_axis=0, tiled=True
    )
    laid = lay(received)
    cache = laid.T.reshape(1, 1, slots * rows, width)

    state = stick(projected, queries, score_offset)
    for distance in (1, 2, 4):
        dtype = jnp.bfloat16 if distance == 4 else jnp.float32
        state = join(state, partner(state, "sp_1", distance), "sp_1", distance, dtype)
    own = jnp.stack([state] + [partner(state, "sp_0", d) for d in (2, 4, 6)])
    other = partner(own, "sp_0", 1)
    read = finish(own, other, seqs, heads)
    return cache, read


def solution(mesh):
    torus = Mesh(
        mesh.devices.reshape(mesh.shape["gr"], 8, 8, mesh.shape["tp"]), ("gr", "sp_0", "sp_1", "tp")
    )
    return jax.shard_map(
        local,
        mesh=torus,
        in_specs=(P(("gr", "tp"), SP, None), P(), P(("gr", "tp"), None), P()),
        out_specs=(P(("gr", "tp"), SP, None, None), P(("gr", "tp"), None)),
        check_vma=False,
    )
```

time: 180 us -> 99 us (0.55)
  blocking collectives: 81.5 us -> 0 us
  starting transfers between devices: 23.3 us -> 59.3 us
  waiting for transfers between devices: 51.2 us -> 27.5 us
  local copies, waits for them, and re-layouts: 13.2 us -> 1.44 us
  Pallas kernels: 0 us -> 9.35 us
  matrix products: 5.16 us -> 0 us
  other arithmetic: 4.79 us -> 0.01 us
    psum x2 -> x0, blocking collectives: 81.5 us -> none  [by_axis(): shard = lax.psum(shard, axis)]
    all_to_all x1, waiting for transfers between devices: 51.2 us -> 0.01 us  [local(): lax.all_to_all(projected.reshape(slots, width, rows), SP, split_axis=0, c...]
    ppermute x1 -> x7, starting transfers between devices: 1.29 us -> 37.3 us  [partner(): lax.ppermute(block, axis, [(i, i ^ distance) for i in range(lax.axis_size...]
    ppermute x1 -> x7, waiting for transfers between devices: 0.01 us -> 27.5 us  [partner(): lax.ppermute(block, axis, [(i, i ^ distance) for i in range(lax.axis_size...]
    pallas_call x0 -> x7, Pallas kernels: none -> 9.35 us  [the longest x1 6.44 us: project(): pl.pallas_call(project_kernel, grid=(features // step,), in_specs=[pl.Blo...]
    unnamed x7 -> x6, local copies, waits for them, and re-layouts: 6.76 us -> 1.23 us
    dot_general x3 -> x0, matrix products: 5.16 us -> none  [the longest x1 4.54 us: local(): jnp.einsum('spd,dcw->scpw', tokens, kv_weight.reshape(model_width, blocks...]
    another operation x2 -> x1, other arithmetic: 4.23 us -> 0.01 us  [local(): own = jnp.stack([state] + [partner(state, 'sp_0', d) for d in (2, 4, 6)])]
  transfers between devices with their start and end apart: 2 -> 8, of which waited for: 1 -> 6; matrix products, arithmetic and copies ran while one was open for 3% -> 0% of each run, Pallas kernels for 0% -> 2%
where the time goes in v1:
time: 99 us; the launch traced here: 98.4 us
  starting transfers between devices  59.3 us (60%)
  waiting for transfers between devices  27.5 us (28%)
  Pallas kernels  9.35 us (9%)
  local copies, waits for them, and re-layouts  1.44 us (1%)
    ppermute x7, starting transfers between devices, partner(): lax.ppermute(block, axis, [(i, i ^ distance) for i in range(lax.axis_size...  37.3 us
    ppermute x7, waiting for transfers between devices, partner(): lax.ppermute(block, axis, [(i, i ^ distance) for i in range(lax.axis_size...  27.5 us
    all_to_all x1, starting transfers between devices, local(): lax.all_to_all(projected.reshape(slots, width, rows), SP, split_axis=0, c...  22 us
    pallas_call x1, Pallas kernels, project(): pl.pallas_call(project_kernel, grid=(features // step,), in_specs=[pl.Blo...  6.44 us
  transfers between devices with their start and end apart: 8, of which 6 were waited for; matrix products, arithmetic and copies ran while one was open for 0% of the time, Pallas kernels for 2%

profile of v1, /device:TPU:6, one launch (start us, length us, event | category | flops | bytes accessed | tf_op | source)
XLA Modules:
  0.0 98.4 jit_solution(17154094295275395634)
XLA Ops:
  0.7 6.4 %project.1.kv_ref = bf16[4,16,64,128]{3,2,1,0:T(8,128)(2,1)} custom-call(bf16[4,128,2048]{2,1,0:T(8,128)(2,1)} %x_ref.1, bf16[2048,1024]{1,0:T(8,128)(2,1)} %w_ref.1), custom_call_target="tpu_custom_call" | custom-call | tf_op jit(solution)/shard_map/project/pallas_call | solution.py:39
  7.1 22.0 %all-to-all-start = ((bf16[64,64,128]{2,1,0:T(8,128)(2,1)}), bf16[64,64,128]{2,1,0:T(8,128)(2,1)S(1)}, u32[]{:S(2)}, u32[]{:S(2)}) async-start(bf16[64,64,128]{2,1,0:T(8,128)(2,1)} %bitcast.9), calls=%async_computation | async-start | bytes 2097152 | tf_op jit(solution)/shard_map/all_to_all | solution.py:205
  29.1 0.1 broadcast_in_dim_tile.4.off_ref
  29.2 0.1 reshape.19
  29.3 0.0 copy-start
  29.3 1.2 %copy-done = bf16[4,16,64,128]{3,2,1,0:T(8,128)(2,1)S(1)} copy-done((bf16[4,16,64,128]{3,2,1,0:T(8,128)(2,1)S(1)}, bf16[4,16,64,128]{3,2,1,0:T(8,128)(2,1)}, u32[]{:S(2)}) %copy-start) | copy-done | bytes 1048600
  30.6 1.0 %stick.1.own_ref = f32[72,128]{1,0:T(8,128)S(1)} custom-call(bf16[4,16,64,128]{3,2,1,0:T(8,128)(2,1)S(1)} %copy-done, bf16[128,64]{1,0:T(8,128)(2,1)S(1)} %bitcast.10, f32[128,1]{1,0:T(8,128)S(1)} %broadcast_in_dim_tile.4.off_ref), custom_call_target="tpu_custom_call" | custom-call | tf_op jit(solution)/shard_map/stick/pallas_call | solution.py:100
  31.6 3.5 %collective-permute-start = (f32[72,128]{1,0:T(8,128)S(1)}, f32[72,128]{1,0:T(8,128)S(1)}, u32[]{:S(2)}, u32[]{:S(2)}) collective-permute-start(f32[72,128]{1,0:T(8,128)S(1)} %stick.1.own_ref), channel_id=1, source_target_pairs={{0,8},{8,0},{16,24},{24,16},{32,40},{40,32},{48,56},{56,48},{1,9},... | collective-permute-start | bytes 110600 | tf_op jit(solution)/shard_map/ppermute | solution.py:111
  35.1 7.1 %collective-permute-done.other_ref = f32[72,128]{1,0:T(8,128)S(1)} collective-permute-done((f32[72,128]{1,0:T(8,128)S(1)}, f32[72,128]{1,0:T(8,128)S(1)}, u32[]{:S(2)}, u32[]{:S(2)}) %collective-permute-start) | collective-permute-done | bytes 36896 | tf_op jit(solution)/shard_map/ppermute | solution.py:111
  42.2 4.6 %collective-permute-start.1 = (f32[72,128]{1,0:T(8,128)S(1)}, f32[72,128]{1,0:T(8,128)S(1)}, u32[]{:S(2)}, u32[]{:S(2)}) collective-permute-start(f32[72,128]{1,0:T(8,128)S(1)} %join.3.own_ref), channel_id=1, source_target_pairs={{0,16},{8,24},{16,0},{24,8},{32,48},{40,56},{48,32},{56,40},{1,17}... | collective-permute-start | bytes 110600 | tf_op jit(solution)/shard_map/ppermute | solution.py:111
  46.9 2.9 %collective-permute-done.1.other_ref = f32[72,128]{1,0:T(8,128)S(1)} collective-permute-done((f32[72,128]{1,0:T(8,128)S(1)}, f32[72,128]{1,0:T(8,128)S(1)}, u32[]{:S(2)}, u32[]{:S(2)}) %collective-permute-start.1) | collective-permute-done | bytes 36896 | tf_op jit(solution)/shard_map/ppermute | solution.py:111
  49.7 6.6 %collective-permute-start.2 = (f32[72,128]{1,0:T(8,128)S(1)}, f32[72,128]{1,0:T(8,128)S(1)}, u32[]{:S(2)}, u32[]{:S(2)}) collective-permute-start(f32[72,128]{1,0:T(8,128)S(1)} %join.4.own_ref), channel_id=1, source_target_pairs={{0,32},{8,40},{16,48},{24,56},{32,0},{40,8},{48,16},{56,24},{1,33}... | collective-permute-start | bytes 110600 | tf_op jit(solution)/shard_map/ppermute | solution.py:111
  56.4 3.8 %collective-permute-done.2.other_ref = f32[72,128]{1,0:T(8,128)S(1)} collective-permute-done((f32[72,128]{1,0:T(8,128)S(1)}, f32[72,128]{1,0:T(8,128)S(1)}, u32[]{:S(2)}, u32[]{:S(2)}) %collective-permute-start.2) | collective-permute-done | bytes 36896 | tf_op jit(solution)/shard_map/ppermute | solution.py:111
  60.2 7.3 %collective-permute-start.3 = (bf16[72,128]{1,0:T(8,128)(2,1)S(1)}, bf16[72,128]{1,0:T(8,128)(2,1)S(1)}, u32[]{:S(2)}, u32[]{:S(2)}) collective-permute-start(bf16[72,128]{1,0:T(8,128)(2,1)S(1)} %join.5), channel_id=1, source_target_pairs={{0,128},{64,192},{128,0},{192,64},{256,384},{320,448},{384,256},{4... | collective-permute-start | bytes 55304 | tf_op jit(solution)/shard_map/ppermute | solution.py:111
  67.5 11.4 %collective-permute-start.4 = (bf16[72,128]{1,0:T(8,128)(2,1)S(1)}, bf16[72,128]{1,0:T(8,128)(2,1)S(1)}, u32[]{:S(2)}, u32[]{:S(2)}) collective-permute-start(bf16[72,128]{1,0:T(8,128)(2,1)S(1)} %join.5), channel_id=1, source_target_pairs={{0,256},{64,320},{128,384},{192,448},{256,0},{320,64},{384,128},{4... | collective-permute-start | bytes 55304 | tf_op jit(solution)/shard_map/ppermute | solution.py:111
  78.9 1.9 %collective-permute-start.5 = (bf16[72,128]{1,0:T(8,128)(2,1)S(1)}, bf16[72,128]{1,0:T(8,128)(2,1)S(1)}, u32[]{:S(2)}, u32[]{:S(2)}) collective-permute-start(bf16[72,128]{1,0:T(8,128)(2,1)S(1)} %join.5), channel_id=1, source_target_pairs={{0,384},{64,448},{128,256},{192,320},{256,128},{320,192},{384,0},{... | collective-permute-start | bytes 55304 | tf_op jit(solution)/shard_map/ppermute | solution.py:111
  80.9 0.0 collective-permute-done.3
  80.9 0.5 collective-permute-done.4
  81.3 9.0 %collective-permute-done.5 = bf16[72,128]{1,0:T(8,128)(2,1)S(1)} collective-permute-done((bf16[72,128]{1,0:T(8,128)(2,1)S(1)}, bf16[72,128]{1,0:T(8,128)(2,1)S(1)}, u32[]{:S(2)}, u32[]{:S(2)}) %collective-permute-start.5) | collective-permute-done | bytes 18464 | tf_op jit(solution)/shard_map/ppermute | solution.py:111
  90.3 1.9 %collective-permute-start.6 = (bf16[4,72,128]{2,1,0:T(8,128)(2,1)S(1)}, bf16[4,72,128]{2,1,0:T(8,128)(2,1)S(1)}, u32[]{:S(2)}, u32[]{:S(2)}) collective-permute-start(bf16[4,72,128]{2,1,0:T(8,128)(2,1)S(1)} %pad_maximum_fusion.own_ref), channel_id=1, source_target_pairs={{0,64},{64,0},{128,192},{192,128},{256,320},{320,256},{384,448},{4... | collective-permute-start | bytes 221192 | tf_op jit(solution)/shard_map/ppermute | solution.py:111
  92.3 4.3 %collective-permute-done.6.other_ref = bf16[4,72,128]{2,1,0:T(8,128)(2,1)S(1)} collective-permute-done((bf16[4,72,128]{2,1,0:T(8,128)(2,1)S(1)}, bf16[4,72,128]{2,1,0:T(8,128)(2,1)S(1)}, u32[]{:S(2)}, u32[]{:S(2)}) %collective-permute-start.6) | collective-permute-done | bytes 73760 | tf_op jit(solution)/shard_map/ppermute | solution.py:111
  96.6 0.9 finish.1
  97.4 0.0 all-to-all-done.in_ref
  97.5 0.9 lay.1
  (11 shorter events, 0.1 us)
Async XLA Ops:
  0.6 28.4 %copy-start.2 = (f32[24]{0:T(128)S(1)}, f32[24]{0:T(128)}, u32[]{:S(2)}) copy-start(f32[24]{0:T(128)} %param.7) | copy-start | bytes 292
  0.6 28.6 %copy-start.1 = (bf16[4,1536]{1,0:T(4,128)(2,1)S(1)}, bf16[4,1536]{1,0:T(4,128)(2,1)}, u32[]{:S(2)}) copy-start(bf16[4,1536]{1,0:T(4,128)(2,1)} %param.6) | copy-start | bytes 36868
  7.1 90.4 %all-to-all-start = ((bf16[64,64,128]{2,1,0:T(8,128)(2,1)}), bf16[64,64,128]{2,1,0:T(8,128)(2,1)S(1)}, u32[]{:S(2)}, u32[]{:S(2)}) async-start(bf16[64,64,128]{2,1,0:T(8,128)(2,1)} %bitcast.9), calls=%async_computation | async-start | bytes 2097152 | tf_op jit(solution)/shard_map/all_to_all | solution.py:205
  29.3 1.2 %copy-start = (bf16[4,16,64,128]{3,2,1,0:T(8,128)(2,1)S(1)}, bf16[4,16,64,128]{3,2,1,0:T(8,128)(2,1)}, u32[]{:S(2)}) copy-start(bf16[4,16,64,128]{3,2,1,0:T(8,128)(2,1)} %project.1.kv_ref) | copy-start | bytes 3145732
  31.6 10.6 %collective-permute-start = (f32[72,128]{1,0:T(8,128)S(1)}, f32[72,128]{1,0:T(8,128)S(1)}, u32[]{:S(2)}, u32[]{:S(2)}) collective-permute-start(f32[72,128]{1,0:T(8,128)S(1)} %stick.1.own_ref), channel_id=1, source_target_pairs={{0,8},{8,0},{16,24},{24,16},{32,40},{40,32},{48,56},{56,48},{1,9},... | collective-permute-start | bytes 110600 | tf_op jit(solution)/shard_map/ppermute | solution.py:111
  42.2 7.5 %collective-permute-start.1 = (f32[72,128]{1,0:T(8,128)S(1)}, f32[72,128]{1,0:T(8,128)S(1)}, u32[]{:S(2)}, u32[]{:S(2)}) collective-permute-start(f32[72,128]{1,0:T(8,128)S(1)} %join.3.own_ref), channel_id=1, source_target_pairs={{0,16},{8,24},{16,0},{24,8},{32,48},{40,56},{48,32},{56,40},{1,17}... | collective-permute-start | bytes 110600 | tf_op jit(solution)/shard_map/ppermute | solution.py:111
  49.7 10.4 %collective-permute-start.2 = (f32[72,128]{1,0:T(8,128)S(1)}, f32[72,128]{1,0:T(8,128)S(1)}, u32[]{:S(2)}, u32[]{:S(2)}) collective-permute-start(f32[72,128]{1,0:T(8,128)S(1)} %join.4.own_ref), channel_id=1, source_target_pairs={{0,32},{8,40},{16,48},{24,56},{32,0},{40,8},{48,16},{56,24},{1,33}... | collective-permute-start | bytes 110600 | tf_op jit(solution)/shard_map/ppermute | solution.py:111
  60.2 20.7 %collective-permute-start.3 = (bf16[72,128]{1,0:T(8,128)(2,1)S(1)}, bf16[72,128]{1,0:T(8,128)(2,1)S(1)}, u32[]{:S(2)}, u32[]{:S(2)}) collective-permute-start(bf16[72,128]{1,0:T(8,128)(2,1)S(1)} %join.5), channel_id=1, source_target_pairs={{0,128},{64,192},{128,0},{192,64},{256,384},{320,448},{384,256},{4... | collective-permute-start | bytes 55304 | tf_op jit(solution)/shard_map/ppermute | solution.py:111
  67.5 13.8 %collective-permute-start.4 = (bf16[72,128]{1,0:T(8,128)(2,1)S(1)}, bf16[72,128]{1,0:T(8,128)(2,1)S(1)}, u32[]{:S(2)}, u32[]{:S(2)}) collective-permute-start(bf16[72,128]{1,0:T(8,128)(2,1)S(1)} %join.5), channel_id=1, source_target_pairs={{0,256},{64,320},{128,384},{192,448},{256,0},{320,64},{384,128},{4... | collective-permute-start | bytes 55304 | tf_op jit(solution)/shard_map/ppermute | solution.py:111
  78.9 11.4 %collective-permute-start.5 = (bf16[72,128]{1,0:T(8,128)(2,1)S(1)}, bf16[72,128]{1,0:T(8,128)(2,1)S(1)}, u32[]{:S(2)}, u32[]{:S(2)}) collective-permute-start(bf16[72,128]{1,0:T(8,128)(2,1)S(1)} %join.5), channel_id=1, source_target_pairs={{0,384},{64,448},{128,256},{192,320},{256,128},{320,192},{384,0},{... | collective-permute-start | bytes 55304 | tf_op jit(solution)/shard_map/ppermute | solution.py:111
  90.3 6.2 %collective-permute-start.6 = (bf16[4,72,128]{2,1,0:T(8,128)(2,1)S(1)}, bf16[4,72,128]{2,1,0:T(8,128)(2,1)S(1)}, u32[]{:S(2)}, u32[]{:S(2)}) collective-permute-start(bf16[4,72,128]{2,1,0:T(8,128)(2,1)S(1)} %pad_maximum_fusion.own_ref), channel_id=1, source_target_pairs={{0,64},{64,0},{128,192},{192,128},{256,320},{320,256},{384,448},{4... | collective-permute-start | bytes 221192 | tf_op jit(solution)/shard_map/ppermute | solution.py:111

commit v2 on v0

v2 whole, which is shorter than its diff:
```python
import functools

import jax
import jax.numpy as jnp
from jax import lax
from jax.experimental import pallas as pl
from jax.experimental.pallas import tpu as pltpu
from jax.sharding import Mesh
from jax.sharding import PartitionSpec as P


KVH = 8
HD = 64
LANES = 128
SLOT = 32
ROWS = HD + 8
DEPTH = 256
SP = ("sp_0", "sp_1")
VMEM = pltpu.VMEM
BF16 = jnp.bfloat16
F32 = jnp.float32
BY_POSITION = (((1,), (1,)), ((), ()))


def pack(values, total):
    high = total.astype(BF16).astype(F32)
    middle = (total - high).astype(BF16).astype(F32)
    row = lax.broadcasted_iota(jnp.int32, total.shape, 0)
    parts = jnp.where(row == 0, high, jnp.where(row == 1, middle, total - high - middle))
    return jnp.concatenate([values, parts], axis=0).astype(BF16)


def unpack(state):
    state = state.astype(F32)
    return state[:HD], state[HD : HD + 1] + state[HD + 1 : HD + 2] + state[HD + 2 : HD + 3]


def fold(first, last):
    return first[0] * jnp.exp(last[1]) + last[0], first[1] + last[1]


def choose(condition, one, other):
    return tuple(jnp.where(condition, a, b) for a, b in zip(one, other))


def head_rows(query_ref, offset_ref, rows):
    seqs = query_ref.shape[0]
    heads = offset_ref.shape[0]
    rows[...] = jnp.zeros_like(rows)
    row = lax.broadcasted_iota(jnp.int32, (SLOT, LANES), 0)
    offset = jnp.zeros((SLOT, LANES), F32)
    for h in range(heads):
        rows[pl.ds(h, seqs, stride=SLOT), :HD] = query_ref[:, h * HD : (h + 1) * HD].astype(F32)
        offset = jnp.where(row == h, offset_ref[h], offset)
    return offset


def split(x, parts):
    pieces = []
    for _ in range(parts):
        piece = x.astype(BF16)
        pieces.append(piece)
        x = x - piece.astype(F32)
    return jnp.concatenate(pieces, axis=0)


def stick(kv, rows, offset, group):
    seqs = kv.shape[0]
    slots = seqs * SLOT
    row_head = lax.broadcasted_iota(jnp.int32, (SLOT, LANES), 0) // group
    logits = []
    for s in range(seqs):
        queries = rows[s * SLOT : (s + 1) * SLOT, :HD].astype(BF16)
        total = jnp.zeros((SLOT, LANES), F32)
        for n in range(KVH):
            part = jnp.dot(queries, kv[s, n], preferred_element_type=F32)
            total = jnp.where(row_head == n, part, total)
        logits.append(total * HD ** (-0.5) + offset)
    logit = jnp.concatenate(logits, axis=0)
    soft = jnp.log1p(jnp.exp(-jnp.abs(logit)))
    log_take = jnp.minimum(logit, 0.0) - soft
    keep = jnp.minimum(-logit, 0.0) - soft
    r = lax.broadcasted_iota(jnp.int32, (LANES, LANES), 0)
    c = lax.broadcasted_iota(jnp.int32, (LANES, LANES), 1)
    sums = jnp.dot(split(keep, 3), (r > c).astype(BF16), preferred_element_type=F32)
    between = sums[:slots] + sums[slots : 2 * slots] + sums[2 * slots :]
    weight = jnp.exp(log_take + between)
    read = []
    for s in range(seqs):
        weights = split(weight[s * SLOT : (s + 1) * SLOT], 2)
        values = kv[s, KVH:].reshape(KVH * HD, LANES)
        product = lax.dot_general(weights, values, BY_POSITION, preferred_element_type=F32)
        product = product[:SLOT] + product[SLOT:]
        halves = [jnp.zeros((SLOT, LANES), F32), jnp.zeros((SLOT, LANES), F32)]
        for n in range(KVH):
            piece = product[:, n // 2 * LANES : (n // 2 + 1) * LANES]
            halves[n % 2] = jnp.where(row_head == n, piece, halves[n % 2])
        read.append(jnp.where(row_head % 2 == 0, halves[0], pltpu.roll(halves[1], HD, 1)))
    total = (between + keep)[:, :1]
    state = jnp.where(c < HD, jnp.concatenate(read, axis=0), total).T
    return pack(state[:HD], state[HD:ROWS])


def project_kernel(
    x_hbm, w_hbm, query_ref, offset_ref, out_hbm, state_ref, x, w, out, rows, x_sem, w_sem, out_sem
):
    seqs, positions, depth = x.shape
    steps = depth // DEPTH
    parts = [pl.ds(i * DEPTH, DEPTH) for i in range(steps)]
    x_in = [pltpu.make_async_copy(x_hbm.at[:, :, p], x.at[:, :, p], x_sem.at[i]) for i, p in enumerate(parts)]
    w_in = [pltpu.make_async_copy(w_hbm.at[p], w.at[p], w_sem.at[i]) for i, p in enumerate(parts)]
    for i in range(steps):
        x_in[i].start()
        w_in[i].start()
    offset = head_rows(query_ref, offset_ref, rows)
    acc = None
    for i in range(steps):
        x_in[i].wait()
        w_in[i].wait()
        part = jnp.dot(
            x[:, :, i * DEPTH : (i + 1) * DEPTH].reshape(seqs * positions, DEPTH),
            w[i * DEPTH : (i + 1) * DEPTH],
            preferred_element_type=F32,
        )
        acc = part if acc is None else acc + part
    copies = []
    for s in range(seqs):
        turned = acc[s * positions : (s + 1) * positions].T
        out[s] = turned.reshape(out.shape[1:]).astype(BF16)
        copies.append(pltpu.make_async_copy(out.at[s], out_hbm.at[s], out_sem.at[s]))
        copies[-1].start()
    state_ref[...] = stick(out, rows, offset, offset_ref.shape[0] // KVH)
    for copy in copies:
        copy.wait()


def project(tokens, kv_weight, queries, score_offset, blocks):
    seqs, positions, depth = tokens.shape
    features = kv_weight.shape[1]
    shape = (seqs, blocks, features // blocks, positions)
    dma = pltpu.SemaphoreType.DMA
    return pl.pallas_call(
        project_kernel,
        in_specs=[
            pl.BlockSpec(memory_space=pl.ANY),
            pl.BlockSpec(memory_space=pl.ANY),
            pl.BlockSpec(memory_space=VMEM),
            pl.BlockSpec(memory_space=pltpu.SMEM),
        ],
        out_specs=[pl.BlockSpec(memory_space=pl.ANY), pl.BlockSpec(memory_space=VMEM)],
        out_shape=[jax.ShapeDtypeStruct(shape, BF16), jax.ShapeDtypeStruct((ROWS, LANES), BF16)],
        scratch_shapes=[
            VMEM(tokens.shape, BF16),
            VMEM(kv_weight.shape, BF16),
            VMEM(shape, BF16),
            VMEM((seqs * SLOT, LANES), F32),
            dma((depth // DEPTH,)),
            dma((depth // DEPTH,)),
            dma((seqs,)),
        ],
        name="project",
    )(tokens, kv_weight, queries, score_offset)


def partner(block, axis, distance):
    return lax.ppermute(block, axis, [(i, i ^ distance) for i in range(lax.axis_size(axis))])


def small(mebibytes):
    return pltpu.CompilerParams(vmem_limit_bytes=mebibytes * 1024 * 1024)


def merge(place, states):
    run = None
    for at in reversed(range(len(states))):
        state = states[0]
        for i in range(1, len(states)):
            state = choose((place ^ at) == i, states[i], state)
        run = state if run is None else fold(state, run)
    return run


def join_kernel(shift, *refs):
    state_refs, out_ref = refs[:-1], refs[-1]
    place = (lax.axis_index("sp_1") >> shift) % len(state_refs)
    for i in range(out_ref.shape[0]):
        values, total = merge(place, [unpack(ref[i]) for ref in state_refs])
        out_ref[i] = pack(values, jnp.broadcast_to(total, (8, LANES)))


def join(runs, shift):
    return pl.pallas_call(
        functools.partial(join_kernel, shift),
        in_specs=[pl.BlockSpec(memory_space=VMEM)] * len(runs),
        out_specs=pl.BlockSpec(memory_space=VMEM),
        out_shape=jax.ShapeDtypeStruct(runs[0].shape, BF16),
        compiler_params=small(2),
        name="join",
    )(*runs)


def finish_kernel(heads, *refs):
    state_refs, (out_ref, turned, wide) = refs[:-3], refs[-3:]
    seqs = out_ref.shape[0]
    states = [unpack(ref[i]) for i in range(2) for ref in state_refs]
    values, _ = merge(lax.axis_index("sp_0"), states)
    turned[...] = jnp.concatenate([values, values], axis=0).T
    for h in range(heads):
        wide[:, h * HD : (h + 1) * HD] = turned[pl.ds(h, seqs, stride=SLOT), :][:, :HD]
    out_ref[...] = wide[...].astype(out_ref.dtype)


def finish(runs, seqs, heads):
    return pl.pallas_call(
        functools.partial(finish_kernel, heads),
        in_specs=[pl.BlockSpec(memory_space=VMEM)] * len(runs),
        out_specs=pl.BlockSpec(memory_space=VMEM),
        out_shape=jax.ShapeDtypeStruct((seqs, heads * HD), BF16),
        scratch_shapes=[VMEM((LANES, LANES), F32), VMEM((seqs, heads * HD), F32)],
        compiler_params=small(2),
        name="finish",
    )(*runs)


def lay_kernel(in_ref, out_ref, sem):
    sources, _, positions = in_ref.shape
    for i in range(sources):
        place = pl.ds(i * positions, positions)
        pltpu.make_async_copy(in_ref.at[i], out_ref.at[:, place], sem).start()
    pltpu.make_async_copy(out_ref, out_ref, sem).wait()


def lay(received):
    sources, width, positions = received.shape
    return pl.pallas_call(
        lay_kernel,
        in_specs=[pl.BlockSpec(memory_space=pl.ANY)],
        out_specs=pl.BlockSpec(memory_space=pl.ANY),
        out_shape=jax.ShapeDtypeStruct((width, sources * positions), received.dtype),
        scratch_shapes=[pltpu.SemaphoreType.DMA],
        compiler_params=small(1),
        name="lay",
    )(received)


def local(tokens, kv_weight, queries, score_offset):
    seqs, positions, _ = tokens.shape
    features = kv_weight.shape[1]
    slots = lax.axis_size(SP)
    blocks = slots // seqs
    width = features // blocks
    heads = score_offset.shape[0]

    projected, state = project(tokens, kv_weight, queries, score_offset, blocks)
    opposite = partner(state, "sp_0", 4)
    received = lax.all_to_all(
        projected.reshape(slots, width, positions), SP, split_axis=0, concat_axis=0, tiled=True
    )
    laid = lay(received)
    cache = laid.T.reshape(1, 1, slots * positions, width)

    runs = jnp.stack([state, opposite])
    runs = join([runs] + [partner(runs, "sp_1", d) for d in (1, 2, 3)], 0)
    runs = join([runs, partner(runs, "sp_1", 4)], 2)
    gathered = [runs]
    for distance in (1, 2, 3):
        gathered.append(partner(runs, "sp_0", distance))
    read = finish(gathered, seqs, heads)
    return cache, read


def solution(mesh):
    torus = Mesh(
        mesh.devices.reshape(mesh.shape["gr"], 8, 8, mesh.shape["tp"]), ("gr", "sp_0", "sp_1", "tp")
    )
    return jax.shard_map(
        local,
        mesh=torus,
        in_specs=(P(("gr", "tp"), SP, None), P(), P(("gr", "tp"), None), P()),
        out_specs=(P(("gr", "tp"), SP, None, None), P(("gr", "tp"), None)),
        check_vma=False,
    )
```

time: 180 us -> 122 us (0.68)
  blocking collectives: 81.5 us -> 0 us
  starting transfers between devices: 23.3 us -> 54.3 us
  local copies, waits for them, and re-layouts: 13.2 us -> 0 us
  Pallas kernels: 0 us -> 8.75 us
  waiting for transfers between devices: 51.2 us -> 56.8 us
  matrix products: 5.16 us -> 0 us
  other arithmetic: 4.79 us -> 0.73 us
    psum x2 -> x0, blocking collectives: 81.5 us -> none  [by_axis(): shard = lax.psum(shard, axis)]
    ppermute x1 -> x8, waiting for transfers between devices: 0.01 us -> 56.8 us  [partner(): lax.ppermute(block, axis, [(i, i ^ distance) for i in range(lax.axis_size...]
    all_to_all x1, waiting for transfers between devices: 51.2 us -> 0.01 us  [local(): lax.all_to_all(projected.reshape(slots, width, positions), SP, split_axis...]
    ppermute x1 -> x8, starting transfers between devices: 1.29 us -> 32.3 us  [partner(): lax.ppermute(block, axis, [(i, i ^ distance) for i in range(lax.axis_size...]
    pallas_call x0 -> x5, Pallas kernels: none -> 8.75 us  [the longest x1 6.72 us: project(): pl.pallas_call(project_kernel, in_specs=[pl.BlockSpec(memory_space=pl.ANY...]
    unnamed x7 -> x0, local copies, waits for them, and re-layouts: 6.76 us -> none
    dot_general x3 -> x0, matrix products: 5.16 us -> none  [the longest x1 4.54 us: local(): jnp.einsum('spd,dcw->scpw', tokens, kv_weight.reshape(model_width, blocks...]
    another operation x2 -> x1, other arithmetic: 4.23 us -> 0.73 us  [local(): runs = jnp.stack([state, opposite])]
  transfers between devices with their start and end apart: 2 -> 9, of which waited for: 1 -> 5; matrix products, arithmetic and copies ran while one was open for 3% -> 1% of each run, Pallas kernels for 0% -> 1%
where the time goes in v2:
time: 122 us; the launch traced here: 121 us
  waiting for transfers between devices  56.8 us (47%)
  starting transfers between devices  54.3 us (45%)
  Pallas kernels  8.75 us (7%)
    ppermute x8, waiting for transfers between devices, partner(): lax.ppermute(block, axis, [(i, i ^ distance) for i in range(lax.axis_size...  56.8 us
    ppermute x8, starting transfers between devices, partner(): lax.ppermute(block, axis, [(i, i ^ distance) for i in range(lax.axis_size...  32.3 us
    all_to_all x1, starting transfers between devices, local(): lax.all_to_all(projected.reshape(slots, width, positions), SP, split_axis...  22 us
    pallas_call x1, Pallas kernels, project(): pl.pallas_call(project_kernel, in_specs=[pl.BlockSpec(memory_space=pl.ANY...  6.72 us
  transfers between devices with their start and end apart: 9, of which 5 were waited for; matrix products, arithmetic and copies ran while one was open for 1% of the time, Pallas kernels for 1%

profile of v2, /device:TPU:6, one launch (start us, length us, event | category | flops | bytes accessed | tf_op | source)
XLA Modules:
  0.0 121.3 jit_solution(2123832026906197671)
XLA Ops:
  0.6 6.7 %project.1 = (bf16[4,16,64,128]{3,2,1,0:T(8,128)(2,1)}, bf16[72,128]{1,0:T(8,128)(2,1)}) custom-call(bf16[4,128,2048]{2,1,0:T(8,128)(2,1)} %x_hbm.1, bf16[2048,1024]{1,0:T(8,128)(2,1)} %w_hbm.1, bf16[4,1536]{1,0:T(4,128)(2,1)} %query_ref.1, f32[24]{0:T(128)} %offset_ref.1), custom_call_target="tpu_custom_call" | custom-call | tf_op jit(solution)/shard_map/project/pallas_call | solution.py:142
  7.4 22.0 %all-to-all-start = ((bf16[64,64,128]{2,1,0:T(8,128)(2,1)}), bf16[64,64,128]{2,1,0:T(8,128)(2,1)S(1)}, u32[]{:S(2)}, u32[]{:S(2)}) async-start(bf16[64,64,128]{2,1,0:T(8,128)(2,1)} %bitcast.6), calls=%async_computation | async-start | bytes 2097152 | tf_op jit(solution)/shard_map/all_to_all | solution.py:256
  29.4 7.5 %collective-permute-start = (bf16[72,128]{1,0:T(8,128)(2,1)}, bf16[72,128]{1,0:T(8,128)(2,1)S(1)}, u32[]{:S(2)}, u32[]{:S(2)}) collective-permute-start(bf16[72,128]{1,0:T(8,128)(2,1)} %get-tuple-element.5), channel_id=1, source_target_pairs={{0,256},{64,320},{128,384},{192,448},{256,0},{320,64},{384,128},{4... | collective-permute-start | bytes 55304 | tf_op jit(solution)/shard_map/ppermute | solution.py:166
  36.9 44.6 %collective-permute-done = bf16[72,128]{1,0:T(8,128)(2,1)S(1)} collective-permute-done((bf16[72,128]{1,0:T(8,128)(2,1)}, bf16[72,128]{1,0:T(8,128)(2,1)S(1)}, u32[]{:S(2)}, u32[]{:S(2)}) %collective-permute-start) | collective-permute-done | bytes 18464 | tf_op jit(solution)/shard_map/ppermute | solution.py:166
  81.4 0.7 pad_maximum_fusion.refs_0_
  82.2 3.4 %collective-permute-start.1 = (bf16[2,72,128]{2,1,0:T(8,128)(2,1)S(1)}, bf16[2,72,128]{2,1,0:T(8,128)(2,1)S(1)}, u32[]{:S(2)}, u32[]{:S(2)}) collective-permute-start(bf16[2,72,128]{2,1,0:T(8,128)(2,1)S(1)} %pad_maximum_fusion.refs_0_), channel_id=1, source_target_pairs={{0,8},{8,0},{16,24},{24,16},{32,40},{40,32},{48,56},{56,48},{1,9},... | collective-permute-start | bytes 110600 | tf_op jit(solution)/shard_map/ppermute | solution.py:166
  85.5 4.3 %collective-permute-start.2 = (bf16[2,72,128]{2,1,0:T(8,128)(2,1)S(1)}, bf16[2,72,128]{2,1,0:T(8,128)(2,1)S(1)}, u32[]{:S(2)}, u32[]{:S(2)}) collective-permute-start(bf16[2,72,128]{2,1,0:T(8,128)(2,1)S(1)} %pad_maximum_fusion.refs_0_), channel_id=1, source_target_pairs={{0,16},{8,24},{16,0},{24,8},{32,48},{40,56},{48,32},{56,40},{1,17}... | collective-permute-start | bytes 110600 | tf_op jit(solution)/shard_map/ppermute | solution.py:166
  89.8 2.5 %collective-permute-start.3 = (bf16[2,72,128]{2,1,0:T(8,128)(2,1)S(1)}, bf16[2,72,128]{2,1,0:T(8,128)(2,1)S(1)}, u32[]{:S(2)}, u32[]{:S(2)}) collective-permute-start(bf16[2,72,128]{2,1,0:T(8,128)(2,1)S(1)} %pad_maximum_fusion.refs_0_), channel_id=1, source_target_pairs={{0,24},{8,16},{16,8},{24,0},{32,56},{40,48},{48,40},{56,32},{1,25}... | collective-permute-start | bytes 110600 | tf_op jit(solution)/shard_map/ppermute | solution.py:166
  92.3 0.0 collective-permute-done.1.refs_1_
  92.3 0.4 collective-permute-done.2.refs_2_
  92.7 4.8 %collective-permute-done.3.refs_3_ = bf16[2,72,128]{2,1,0:T(8,128)(2,1)S(1)} collective-permute-done((bf16[2,72,128]{2,1,0:T(8,128)(2,1)S(1)}, bf16[2,72,128]{2,1,0:T(8,128)(2,1)S(1)}, u32[]{:S(2)}, u32[]{:S(2)}) %collective-permute-start.3) | collective-permute-done | bytes 36896 | tf_op jit(solution)/shard_map/ppermute | solution.py:166
  97.5 0.1 join.2.refs_0_
  97.6 4.6 %collective-permute-start.4 = (bf16[2,72,128]{2,1,0:T(8,128)(2,1)S(1)}, bf16[2,72,128]{2,1,0:T(8,128)(2,1)S(1)}, u32[]{:S(2)}, u32[]{:S(2)}) collective-permute-start(bf16[2,72,128]{2,1,0:T(8,128)(2,1)S(1)} %join.2.refs_0_), channel_id=1, source_target_pairs={{0,32},{8,40},{16,48},{24,56},{32,0},{40,8},{48,16},{56,24},{1,33}... | collective-permute-start | bytes 110600 | tf_op jit(solution)/shard_map/ppermute | solution.py:166
  102.2 5.2 %collective-permute-done.4.refs_1_ = bf16[2,72,128]{2,1,0:T(8,128)(2,1)S(1)} collective-permute-done((bf16[2,72,128]{2,1,0:T(8,128)(2,1)S(1)}, bf16[2,72,128]{2,1,0:T(8,128)(2,1)S(1)}, u32[]{:S(2)}, u32[]{:S(2)}) %collective-permute-start.4) | collective-permute-done | bytes 36896 | tf_op jit(solution)/shard_map/ppermute | solution.py:166
  107.4 1.9 %collective-permute-start.5 = (bf16[2,72,128]{2,1,0:T(8,128)(2,1)S(1)}, bf16[2,72,128]{2,1,0:T(8,128)(2,1)S(1)}, u32[]{:S(2)}, u32[]{:S(2)}) collective-permute-start(bf16[2,72,128]{2,1,0:T(8,128)(2,1)S(1)} %join.3.refs_0_), channel_id=1, source_target_pairs={{0,64},{64,0},{128,192},{192,128},{256,320},{320,256},{384,448},{4... | collective-permute-start | bytes 110600 | tf_op jit(solution)/shard_map/ppermute | solution.py:166
  109.3 1.9 %collective-permute-start.6 = (bf16[2,72,128]{2,1,0:T(8,128)(2,1)S(1)}, bf16[2,72,128]{2,1,0:T(8,128)(2,1)S(1)}, u32[]{:S(2)}, u32[]{:S(2)}) collective-permute-start(bf16[2,72,128]{2,1,0:T(8,128)(2,1)S(1)} %join.3.refs_0_), channel_id=1, source_target_pairs={{0,128},{64,192},{128,0},{192,64},{256,384},{320,448},{384,256},{4... | collective-permute-start | bytes 110600 | tf_op jit(solution)/shard_map/ppermute | solution.py:166
  111.2 6.3 %collective-permute-start.7 = (bf16[2,72,128]{2,1,0:T(8,128)(2,1)S(1)}, bf16[2,72,128]{2,1,0:T(8,128)(2,1)S(1)}, u32[]{:S(2)}, u32[]{:S(2)}) collective-permute-start(bf16[2,72,128]{2,1,0:T(8,128)(2,1)S(1)} %join.3.refs_0_), channel_id=1, source_target_pairs={{0,192},{64,128},{128,64},{192,0},{256,448},{320,384},{384,320},{4... | collective-permute-start | bytes 110600 | tf_op jit(solution)/shard_map/ppermute | solution.py:166
  117.5 0.0 collective-permute-done.5.refs_1_
  117.5 0.0 collective-permute-done.6.refs_2_
  117.5 1.9 %collective-permute-done.7.refs_3_ = bf16[2,72,128]{2,1,0:T(8,128)(2,1)S(1)} collective-permute-done((bf16[2,72,128]{2,1,0:T(8,128)(2,1)S(1)}, bf16[2,72,128]{2,1,0:T(8,128)(2,1)S(1)}, u32[]{:S(2)}, u32[]{:S(2)}) %collective-permute-start.7) | collective-permute-done | bytes 36896 | tf_op jit(solution)/shard_map/ppermute | solution.py:166
  119.4 1.0 finish.1
  120.4 0.0 all-to-all-done.in_ref
  120.4 0.9 lay.1
  (1 shorter events, 0.0 us)
Async XLA Ops:
  7.4 113.0 %all-to-all-start = ((bf16[64,64,128]{2,1,0:T(8,128)(2,1)}), bf16[64,64,128]{2,1,0:T(8,128)(2,1)S(1)}, u32[]{:S(2)}, u32[]{:S(2)}) async-start(bf16[64,64,128]{2,1,0:T(8,128)(2,1)} %bitcast.6), calls=%async_computation | async-start | bytes 2097152 | tf_op jit(solution)/shard_map/all_to_all | solution.py:256
  29.4 52.1 %collective-permute-start = (bf16[72,128]{1,0:T(8,128)(2,1)}, bf16[72,128]{1,0:T(8,128)(2,1)S(1)}, u32[]{:S(2)}, u32[]{:S(2)}) collective-permute-start(bf16[72,128]{1,0:T(8,128)(2,1)} %get-tuple-element.5), channel_id=1, source_target_pairs={{0,256},{64,320},{128,384},{192,448},{256,0},{320,64},{384,128},{4... | collective-permute-start | bytes 55304 | tf_op jit(solution)/shard_map/ppermute | solution.py:166
  82.2 10.1 %collective-permute-start.1 = (bf16[2,72,128]{2,1,0:T(8,128)(2,1)S(1)}, bf16[2,72,128]{2,1,0:T(8,128)(2,1)S(1)}, u32[]{:S(2)}, u32[]{:S(2)}) collective-permute-start(bf16[2,72,128]{2,1,0:T(8,128)(2,1)S(1)} %pad_maximum_fusion.refs_0_), channel_id=1, source_target_pairs={{0,8},{8,0},{16,24},{24,16},{32,40},{40,32},{48,56},{56,48},{1,9},... | collective-permute-start | bytes 110600 | tf_op jit(solution)/shard_map/ppermute | solution.py:166
  85.5 7.1 %collective-permute-start.2 = (bf16[2,72,128]{2,1,0:T(8,128)(2,1)S(1)}, bf16[2,72,128]{2,1,0:T(8,128)(2,1)S(1)}, u32[]{:S(2)}, u32[]{:S(2)}) collective-permute-start(bf16[2,72,128]{2,1,0:T(8,128)(2,1)S(1)} %pad_maximum_fusion.refs_0_), channel_id=1, source_target_pairs={{0,16},{8,24},{16,0},{24,8},{32,48},{40,56},{48,32},{56,40},{1,17}... | collective-permute-start | bytes 110600 | tf_op jit(solution)/shard_map/ppermute | solution.py:166
  89.8 7.7 %collective-permute-start.3 = (bf16[2,72,128]{2,1,0:T(8,128)(2,1)S(1)}, bf16[2,72,128]{2,1,0:T(8,128)(2,1)S(1)}, u32[]{:S(2)}, u32[]{:S(2)}) collective-permute-start(bf16[2,72,128]{2,1,0:T(8,128)(2,1)S(1)} %pad_maximum_fusion.refs_0_), channel_id=1, source_target_pairs={{0,24},{8,16},{16,8},{24,0},{32,56},{40,48},{48,40},{56,32},{1,25}... | collective-permute-start | bytes 110600 | tf_op jit(solution)/shard_map/ppermute | solution.py:166
  97.6 9.8 %collective-permute-start.4 = (bf16[2,72,128]{2,1,0:T(8,128)(2,1)S(1)}, bf16[2,72,128]{2,1,0:T(8,128)(2,1)S(1)}, u32[]{:S(2)}, u32[]{:S(2)}) collective-permute-start(bf16[2,72,128]{2,1,0:T(8,128)(2,1)S(1)} %join.2.refs_0_), channel_id=1, source_target_pairs={{0,32},{8,40},{16,48},{24,56},{32,0},{40,8},{48,16},{56,24},{1,33}... | collective-permute-start | bytes 110600 | tf_op jit(solution)/shard_map/ppermute | solution.py:166
  107.4 10.1 %collective-permute-start.5 = (bf16[2,72,128]{2,1,0:T(8,128)(2,1)S(1)}, bf16[2,72,128]{2,1,0:T(8,128)(2,1)S(1)}, u32[]{:S(2)}, u32[]{:S(2)}) collective-permute-start(bf16[2,72,128]{2,1,0:T(8,128)(2,1)S(1)} %join.3.refs_0_), channel_id=1, source_target_pairs={{0,64},{64,0},{128,192},{192,128},{256,320},{320,256},{384,448},{4... | collective-permute-start | bytes 110600 | tf_op jit(solution)/shard_map/ppermute | solution.py:166
  109.3 8.2 %collective-permute-start.6 = (bf16[2,72,128]{2,1,0:T(8,128)(2,1)S(1)}, bf16[2,72,128]{2,1,0:T(8,128)(2,1)S(1)}, u32[]{:S(2)}, u32[]{:S(2)}) collective-permute-start(bf16[2,72,128]{2,1,0:T(8,128)(2,1)S(1)} %join.3.refs_0_), channel_id=1, source_target_pairs={{0,128},{64,192},{128,0},{192,64},{256,384},{320,448},{384,256},{4... | collective-permute-start | bytes 110600 | tf_op jit(solution)/shard_map/ppermute | solution.py:166
  111.2 8.2 %collective-permute-start.7 = (bf16[2,72,128]{2,1,0:T(8,128)(2,1)S(1)}, bf16[2,72,128]{2,1,0:T(8,128)(2,1)S(1)}, u32[]{:S(2)}, u32[]{:S(2)}) collective-permute-start(bf16[2,72,128]{2,1,0:T(8,128)(2,1)S(1)} %join.3.refs_0_), channel_id=1, source_target_pairs={{0,192},{64,128},{128,64},{192,0},{256,448},{320,384},{384,320},{4... | collective-permute-start | bytes 110600 | tf_op jit(solution)/shard_map/ppermute | solution.py:166

commit v3 on v2

--- a/solution.py
+++ b/solution.py
@@ -13,6 +13,7 @@
 HD = 64
 LANES = 128
 SLOT = 32
+SIDE = 8
 ROWS = HD + 8
 DEPTH = 256
 SP = ("sp_0", "sp_1")
@@ -102,7 +103,20 @@
 
 
 def project_kernel(
-    x_hbm, w_hbm, query_ref, offset_ref, out_hbm, state_ref, x, w, out, rows, x_sem, w_sem, out_sem
+    x_hbm,
+    w_hbm,
+    query_ref,
+    offset_ref,
+    out_hbm,
+    keep_ref,
+    send_ref,
+    x,
+    w,
+    out,
+    rows,
+    x_sem,
+    w_sem,
+    out_sem,
 ):
     seqs, positions, depth = x.shape
     steps = depth // DEPTH
@@ -127,9 +141,20 @@
     for s in range(seqs):
         turned = acc[s * positions : (s + 1) * positions].T
         out[s] = turned.reshape(out.shape[1:]).astype(BF16)
-        copies.append(pltpu.make_async_copy(out.at[s], out_hbm.at[s], out_sem.at[s]))
+        rest = out.at[s, :, pl.ds(SIDE, out.shape[2] - SIDE)]
+        copies.append(pltpu.make_async_copy(rest, out_hbm.at[s], out_sem.at[s]))
         copies[-1].start()
-    state_ref[...] = stick(out, rows, offset, offset_ref.shape[0] // KVH)
+    slots = seqs * out.shape[1]
+    half = slots // 2
+    me = slot()
+    for r in range(slots):
+        to = me ^ r
+        at = ROWS + r % half * SIDE
+        side_ref = send_ref if r >= half else keep_ref
+        side_ref[at : at + SIDE] = out[to // out.shape[1], to % out.shape[1], :SIDE]
+    state = stick(out, rows, offset, offset_ref.shape[0] // KVH)
+    keep_ref[:ROWS] = state
+    send_ref[:ROWS] = state
     for copy in copies:
         copy.wait()
 
@@ -138,17 +163,19 @@
     seqs, positions, depth = tokens.shape
     features = kv_weight.shape[1]
     shape = (seqs, blocks, features // blocks, positions)
+    rest = (seqs, blocks, features // blocks - SIDE, positions)
+    side = jax.ShapeDtypeStruct((ROWS + seqs * blocks // 2 * SIDE, LANES), BF16)
     dma = pltpu.SemaphoreType.DMA
     return pl.pallas_call(
         project_kernel,
         in_specs=[
-            pl.BlockSpec(memory_space=pl.ANY),
-            pl.BlockSpec(memory_space=pl.ANY),
+            pl.BlockSpec(memory_space=pltpu.HBM),
+            pl.BlockSpec(memory_space=pltpu.HBM),
             pl.BlockSpec(memory_space=VMEM),
             pl.BlockSpec(memory_space=pltpu.SMEM),
         ],
-        out_specs=[pl.BlockSpec(memory_space=pl.ANY), pl.BlockSpec(memory_space=VMEM)],
-        out_shape=[jax.ShapeDtypeStruct(shape, BF16), jax.ShapeDtypeStruct((ROWS, LANES), BF16)],
+        out_specs=[pl.BlockSpec(memory_space=pltpu.HBM)] + [pl.BlockSpec(memory_space=VMEM)] * 2,
+        out_shape=[jax.ShapeDtypeStruct(rest, BF16), side, side],
         scratch_shapes=[
             VMEM(tokens.shape, BF16),
             VMEM(kv_weight.shape, BF16),
@@ -162,6 +189,10 @@
     )(tokens, kv_weight, queries, score_offset)
 
 
+def slot():
+    return lax.axis_index("sp_0") * 8 + lax.axis_index("sp_1")
+
+
 def partner(block, axis, distance):
     return lax.ppermute(block, axis, [(i, i ^ distance) for i in range(lax.axis_size(axis))])
 
@@ -180,54 +211,121 @@
     return run
 
 
-def join_kernel(shift, *refs):
-    state_refs, out_ref = refs[:-1], refs[-1]
-    place = (lax.axis_index("sp_1") >> shift) % len(state_refs)
-    for i in range(out_ref.shape[0]):
-        values, total = merge(place, [unpack(ref[i]) for ref in state_refs])
-        out_ref[i] = pack(values, jnp.broadcast_to(total, (8, LANES)))
-
-
-def join(runs, shift):
+def states_of(ref):
+    return [unpack(ref[i * ROWS : (i + 1) * ROWS]) for i in range(2)]
+
+
+def move(from_ref, source, to_ref, target, base):
+    to_ref[2 * ROWS + target * SIDE : 2 * ROWS + (target + 1) * SIDE] = from_ref[
+        base + source * SIDE : base + (source + 1) * SIDE
+    ]
+
+
+def pair_kernel(*refs):
+    in_refs, out_refs = refs[:2], refs[2:]
+    for low, out_ref in enumerate(out_refs):
+        for i, in_ref in enumerate(in_refs):
+            out_ref[i * ROWS : (i + 1) * ROWS] = in_ref[:ROWS]
+            for z in range(4):
+                for high in range(2):
+                    move(in_ref, z * 8 + high * 4 + low, out_ref, i * 8 + z * 2 + high, ROWS)
+
+
+def join_low_kernel(*refs):
+    in_refs, out_refs = refs[:4], refs[4:]
+    found = [states_of(ref) for ref in in_refs]
+    place = lax.axis_index("sp_1") % 4
+    for i in range(2):
+        values, total = merge(place, [states[i] for states in found])
+        state = pack(values, jnp.broadcast_to(total, (8, LANES)))
+        for out_ref in out_refs:
+            out_ref[i * ROWS : (i + 1) * ROWS] = state
+    for high, out_ref in enumerate(out_refs):
+        for low, in_ref in enumerate(in_refs):
+            for i in range(2):
+                for z in range(4):
+                    move(in_ref, i * 8 + z * 2 + high, out_ref, low * 8 + i * 4 + z, 2 * ROWS)
+
+
+def join_high_kernel(*refs):
+    in_refs, out_refs = refs[:2], refs[2:]
+    found = [states_of(ref) for ref in in_refs]
+    place = lax.axis_index("sp_1") // 4
+    for i in range(2):
+        values, total = merge(place, [states[i] for states in found])
+        state = pack(values, jnp.broadcast_to(total, (8, LANES)))
+        for out_ref in out_refs:
+            out_ref[i * ROWS : (i + 1) * ROWS] = state
+    for z, out_ref in enumerate(out_refs):
+        for high, in_ref in enumerate(in_refs):
+            for low in range(4):
+                for i in range(2):
+                    move(in_ref, low * 8 + i * 4 + z, out_ref, high * 8 + low * 2 + i, 2 * ROWS)
+
+
+def exchange(kernel, arrived, count):
+    shape = jax.ShapeDtypeStruct((2 * ROWS + 64 // count * SIDE, LANES), BF16)
     return pl.pallas_call(
-        functools.partial(join_kernel, shift),
-        in_specs=[pl.BlockSpec(memory_space=VMEM)] * len(runs),
-        out_specs=pl.BlockSpec(memory_space=VMEM),
-        out_shape=jax.ShapeDtypeStruct(runs[0].shape, BF16),
-        compiler_params=small(2),
-        name="join",
-    )(*runs)
+        kernel,
+        in_specs=[pl.BlockSpec(memory_space=VMEM)] * len(arrived),
+        out_specs=[pl.BlockSpec(memory_space=VMEM)] * count,
+        out_shape=[shape] * count,
+        compiler_params=small(3),
+    )(*arrived)
 
 
 def finish_kernel(heads, *refs):
-    state_refs, (out_ref, turned, wide) = refs[:-3], refs[-3:]
+    in_refs, (out_ref, cache_hbm, turned, wide, side, sem) = refs[:4], refs[5:]
     seqs = out_ref.shape[0]
-    states = [unpack(ref[i]) for i in range(2) for ref in state_refs]
-    values, _ = merge(lax.axis_index("sp_0"), states)
+    me = slot()
+    for z, in_ref in enumerate(in_refs):
+        for high in range(2):
+            for low in range(4):
+                for i in range(2):
+                    at = 2 * ROWS + (high * 8 + low * 2 + i) * SIDE
+                    source = me ^ (i * 32 + z * 8 + high * 4 + low)
+                    place = pl.ds(pl.multiple_of(source * LANES, LANES), LANES)
+                    side[:, place] = in_ref[at : at + SIDE]
+    copy = pltpu.make_async_copy(side, cache_hbm.at[pl.ds(0, SIDE)], sem)
+    copy.start()
+    found = [states_of(ref) for ref in in_refs]
+    values, _ = merge(lax.axis_index("sp_0"), [states[i] for i in range(2) for states in found])
     turned[...] = jnp.concatenate([values, values], axis=0).T
     for h in range(heads):
         wide[:, h * HD : (h + 1) * HD] = turned[pl.ds(h, seqs, stride=SLOT), :][:, :HD]
     out_ref[...] = wide[...].astype(out_ref.dtype)
-
-
-def finish(runs, seqs, heads):
+    copy.wait()
+
+
+def finish(arrived, laid, seqs, heads):
     return pl.pallas_call(
         functools.partial(finish_kernel, heads),
-        in_specs=[pl.BlockSpec(memory_space=VMEM)] * len(runs),
-        out_specs=pl.BlockSpec(memory_space=VMEM),
-        out_shape=jax.ShapeDtypeStruct((seqs, heads * HD), BF16),
-        scratch_shapes=[VMEM((LANES, LANES), F32), VMEM((seqs, heads * HD), F32)],
-        compiler_params=small(2),
+        in_specs=[pl.BlockSpec(memory_space=VMEM)] * len(arrived)
+        + [pl.BlockSpec(memory_space=pl.ANY)],
+        out_specs=[pl.BlockSpec(memory_space=VMEM), pl.BlockSpec(memory_space=pl.ANY)],
+        out_shape=[
+            jax.ShapeDtypeStruct((seqs, heads * HD), BF16),
+            jax.ShapeDtypeStruct(laid.shape, BF16),
+        ],
+        scratch_shapes=[
+            VMEM((LANES, LANES), F32),
+            VMEM((seqs, heads * HD), F32),
+            VMEM((SIDE, laid.shape[1]), BF16),
+            pltpu.SemaphoreType.DMA,
+        ],
+        input_output_aliases={len(arrived): 1},
+        compiler_params=small(3),
         name="finish",
-    )(*runs)
+    )(*arrived, laid)
 
 
 def lay_kernel(in_ref, out_ref, sem):
-    sources, _, positions = in_ref.shape
+    sources, width, positions = in_ref.shape
+    rest = pl.ds(SIDE, width)
     for i in range(sources):
         place = pl.ds(i * positions, positions)
-        pltpu.make_async_copy(in_ref.at[i], out_ref.at[:, place], sem).start()
-    pltpu.make_async_copy(out_ref, out_ref, sem).wait()
+        pltpu.make_async_copy(in_ref.at[i], out_ref.at[rest, place], sem).start()
+    pltpu.make_async_copy(out_ref.at[rest], out_ref.at[rest], sem).wait()
 
 
 def lay(received):
@@ -236,7 +334,7 @@
         lay_kernel,
         in_specs=[pl.BlockSpec(memory_space=pl.ANY)],
         out_specs=pl.BlockSpec(memory_space=pl.ANY),
-        out_shape=jax.ShapeDtypeStruct((width, sources * positions), received.dtype),
+        out_shape=jax.ShapeDtypeStruct((SIDE + width, sources * positions), received.dtype),
         scratch_shapes=[pltpu.SemaphoreType.DMA],
         compiler_params=small(1),
         name="lay",
@@ -251,22 +349,26 @@
     width = features // blocks
     heads = score_offset.shape[0]
 
-    projected, state = project(tokens, kv_weight, queries, score_offset, blocks)
-    opposite = partner(state, "sp_0", 4)
+    projected, keep, send = project(tokens, kv_weight, queries, score_offset, blocks)
+    opposite = partner(send, "sp_0", 4)
     received = lax.all_to_all(
-        projected.reshape(slots, width, positions), SP, split_axis=0, concat_axis=0, tiled=True
+        projected.reshape(slots, width - SIDE, positions),
+        SP,
+        split_axis=0,
+        concat_axis=0,
+        tiled=True,
     )
     laid = lay(received)
-    cache = laid.T.reshape(1, 1, slots * positions, width)
-
-    runs = jnp.stack([state, opposite])
-    runs = join([runs] + [partner(runs, "sp_1", d) for d in (1, 2, 3)], 0)
-    runs = join([runs, partner(runs, "sp_1", 4)], 2)
-    gathered = [runs]
+    parts = exchange(pair_kernel, [keep, opposite], 4)
+    parts = [parts[0]] + [partner(parts[d], "sp_1", d) for d in (1, 2, 3)]
+    parts = exchange(join_low_kernel, parts, 2)
+    parts = [parts[0]] + [partner(parts[1], "sp_1", 4)]
+    parts = exchange(join_high_kernel, parts, 4)
+    arrived = [parts[0]]
     for distance in (1, 2, 3):
-        gathered.append(partner(runs, "sp_0", distance))
-    read = finish(gathered, seqs, heads)
-    return cache, read
+        arrived.append(partner(parts[distance], "sp_0", distance))
+    read, cache = finish(arrived, laid, seqs, heads)
+    return cache.T.reshape(1, 1, slots * positions, width), read
 
 
 def solution(mesh):

time: 122 us -> 124 us (1.016)
  waiting for transfers between devices: 56.8 us -> 58.4 us
    ppermute x8, waiting for transfers between devices: 56.8 us -> 58.4 us  [partner(): lax.ppermute(block, axis, [(i, i ^ distance) for i in range(lax.axis_size...]
    pallas_call x3 -> x4, Pallas kernels: 6.84 us -> 6.78 us  [the longest x1 6.59 us: project(): pl.pallas_call(project_kernel, in_specs=[pl.BlockSpec(memory_space=pltpu....]
  transfers between devices with their start and end apart: 9 -> 9, of which waited for: 5 -> 5; matrix products, arithmetic and copies ran while one was open for 1% -> 0% of each run, Pallas kernels for 1% -> 1%
where the time goes in v3:
time: 124 us
  waiting for transfers between devices  58.4 us (47%)
  starting transfers between devices  54.4 us (44%)
  Pallas kernels  9.26 us (7%)
    ppermute x8, waiting for transfers between devices, partner(): lax.ppermute(block, axis, [(i, i ^ distance) for i in range(lax.axis_size...  58.4 us
    ppermute x8, starting transfers between devices, partner(): lax.ppermute(block, axis, [(i, i ^ distance) for i in range(lax.axis_size...  32.4 us
    all_to_all x1, starting transfers between devices, local(): lax.all_to_all(projected.reshape(slots, width - SIDE, positions), SP, spl...  22 us
    pallas_call x1, Pallas kernels, project(): pl.pallas_call(project_kernel, in_specs=[pl.BlockSpec(memory_space=pltpu....  6.59 us
  transfers between devices with their start and end apart: 9, of which 5 were waited for; matrix products, arithmetic and copies ran while one was open for 0% of the time, Pallas kernels for 1%

profile of v3, /device:TPU:6, one launch (start us, length us, event | category | flops | bytes accessed | tf_op | source)
XLA Modules:
  0.0 123.6 jit_solution(10190818035503779564)
XLA Ops:
  0.6 6.6 %project.1 = (bf16[4,16,56,128]{3,2,1,0:T(8,128)(2,1)}, bf16[328,128]{1,0:T(8,128)(2,1)}, bf16[328,128]{1,0:T(8,128)(2,1)}) custom-call(bf16[4,128,2048]{2,1,0:T(8,128)(2,1)} %x_hbm.1, bf16[2048,1024]{1,0:T(8,128)(2,1)} %w_hbm.1, bf16[4,1536]{1,0:T(4,128)(2,1)} %query_ref.1, f32[24]{0:T(128)} %offset_ref.1), custom_call_target="tpu_custom_call" | custom-call | tf_op jit(solution)/shard_map/project/pallas_call | solution.py:169
  7.2 22.0 %all-to-all-start = ((bf16[64,56,128]{2,1,0:T(8,128)(2,1)}), bf16[64,56,128]{2,1,0:T(8,128)(2,1)S(1)}, u32[]{:S(2)}, u32[]{:S(2)}) async-start(bf16[64,56,128]{2,1,0:T(8,128)(2,1)} %bitcast.5), calls=%async_computation | async-start | bytes 1835008 | tf_op jit(solution)/shard_map/all_to_all | solution.py:354
  29.2 7.5 %collective-permute-start = (bf16[328,128]{1,0:T(8,128)(2,1)}, bf16[328,128]{1,0:T(8,128)(2,1)S(1)}, u32[]{:S(2)}, u32[]{:S(2)}) collective-permute-start(bf16[328,128]{1,0:T(8,128)(2,1)} %get-tuple-element.18), channel_id=1, source_target_pairs={{0,256},{64,320},{128,384},{192,448},{256,0},{320,64},{384,128},{4... | collective-permute-start | bytes 251912 | tf_op jit(solution)/shard_map/ppermute | solution.py:197
  36.7 44.6 %collective-permute-done.refs_1_ = bf16[328,128]{1,0:T(8,128)(2,1)S(1)} collective-permute-done((bf16[328,128]{1,0:T(8,128)(2,1)}, bf16[328,128]{1,0:T(8,128)(2,1)S(1)}, u32[]{:S(2)}, u32[]{:S(2)}) %collective-permute-start) | collective-permute-done | bytes 84000 | tf_op jit(solution)/shard_map/ppermute | solution.py:197
  81.3 0.9 copy-done
  82.2 3.4 %collective-permute-start.1 = (bf16[272,128]{1,0:T(8,128)(2,1)S(1)}, bf16[272,128]{1,0:T(8,128)(2,1)S(1)}, u32[]{:S(2)}, u32[]{:S(2)}) collective-permute-start(bf16[272,128]{1,0:T(8,128)(2,1)S(1)} %get-tuple-element.20), channel_id=1, source_target_pairs={{0,8},{8,0},{16,24},{24,16},{32,40},{40,32},{48,56},{56,48},{1,9},... | collective-permute-start | bytes 208904 | tf_op jit(solution)/shard_map/ppermute | solution.py:197
  85.6 4.3 %collective-permute-start.2 = (bf16[272,128]{1,0:T(8,128)(2,1)S(1)}, bf16[272,128]{1,0:T(8,128)(2,1)S(1)}, u32[]{:S(2)}, u32[]{:S(2)}) collective-permute-start(bf16[272,128]{1,0:T(8,128)(2,1)S(1)} %get-tuple-element.21), channel_id=1, source_target_pairs={{0,16},{8,24},{16,0},{24,8},{32,48},{40,56},{48,32},{56,40},{1,17}... | collective-permute-start | bytes 208904 | tf_op jit(solution)/shard_map/ppermute | solution.py:197
  89.9 2.5 %collective-permute-start.3 = (bf16[272,128]{1,0:T(8,128)(2,1)S(1)}, bf16[272,128]{1,0:T(8,128)(2,1)S(1)}, u32[]{:S(2)}, u32[]{:S(2)}) collective-permute-start(bf16[272,128]{1,0:T(8,128)(2,1)S(1)} %get-tuple-element.22), channel_id=1, source_target_pairs={{0,24},{8,16},{16,8},{24,0},{32,56},{40,48},{48,40},{56,32},{1,25}... | collective-permute-start | bytes 208904 | tf_op jit(solution)/shard_map/ppermute | solution.py:197
  92.4 0.0 collective-permute-done.1.refs_1_
  92.4 1.7 %collective-permute-done.2.refs_2_ = bf16[272,128]{1,0:T(8,128)(2,1)S(1)} collective-permute-done((bf16[272,128]{1,0:T(8,128)(2,1)S(1)}, bf16[272,128]{1,0:T(8,128)(2,1)S(1)}, u32[]{:S(2)}, u32[]{:S(2)}) %collective-permute-start.2) | collective-permute-done | bytes 69664 | tf_op jit(solution)/shard_map/ppermute | solution.py:197
  94.1 3.8 %collective-permute-done.3.refs_3_ = bf16[272,128]{1,0:T(8,128)(2,1)S(1)} collective-permute-done((bf16[272,128]{1,0:T(8,128)(2,1)S(1)}, bf16[272,128]{1,0:T(8,128)(2,1)S(1)}, u32[]{:S(2)}, u32[]{:S(2)}) %collective-permute-start.3) | collective-permute-done | bytes 69664 | tf_op jit(solution)/shard_map/ppermute | solution.py:197
  97.9 0.1 shard_map.60
  98.0 4.7 %collective-permute-start.4 = (bf16[400,128]{1,0:T(8,128)(2,1)S(1)}, bf16[400,128]{1,0:T(8,128)(2,1)S(1)}, u32[]{:S(2)}, u32[]{:S(2)}) collective-permute-start(bf16[400,128]{1,0:T(8,128)(2,1)S(1)} %get-tuple-element.24), channel_id=1, source_target_pairs={{0,32},{8,40},{16,48},{24,56},{32,0},{40,8},{48,16},{56,24},{1,33}... | collective-permute-start | bytes 307208 | tf_op jit(solution)/shard_map/ppermute | solution.py:197
  102.7 6.9 %collective-permute-done.4.refs_1_ = bf16[400,128]{1,0:T(8,128)(2,1)S(1)} collective-permute-done((bf16[400,128]{1,0:T(8,128)(2,1)S(1)}, bf16[400,128]{1,0:T(8,128)(2,1)S(1)}, u32[]{:S(2)}, u32[]{:S(2)}) %collective-permute-start.4) | collective-permute-done | bytes 102432 | tf_op jit(solution)/shard_map/ppermute | solution.py:197
  109.6 0.1 shard_map.61
  109.6 1.9 %collective-permute-start.5 = (bf16[272,128]{1,0:T(8,128)(2,1)S(1)}, bf16[272,128]{1,0:T(8,128)(2,1)S(1)}, u32[]{:S(2)}, u32[]{:S(2)}) collective-permute-start(bf16[272,128]{1,0:T(8,128)(2,1)S(1)} %get-tuple-element.26), channel_id=1, source_target_pairs={{0,64},{64,0},{128,192},{192,128},{256,320},{320,256},{384,448},{4... | collective-permute-start | bytes 208904 | tf_op jit(solution)/shard_map/ppermute | solution.py:197
  111.5 1.9 %collective-permute-start.6 = (bf16[272,128]{1,0:T(8,128)(2,1)S(1)}, bf16[272,128]{1,0:T(8,128)(2,1)S(1)}, u32[]{:S(2)}, u32[]{:S(2)}) collective-permute-start(bf16[272,128]{1,0:T(8,128)(2,1)S(1)} %get-tuple-element.27), channel_id=1, source_target_pairs={{0,128},{64,192},{128,0},{192,64},{256,384},{320,448},{384,256},{4... | collective-permute-start | bytes 208904 | tf_op jit(solution)/shard_map/ppermute | solution.py:197
  113.5 6.3 %collective-permute-start.7 = (bf16[272,128]{1,0:T(8,128)(2,1)S(1)}, bf16[272,128]{1,0:T(8,128)(2,1)S(1)}, u32[]{:S(2)}, u32[]{:S(2)}) collective-permute-start(bf16[272,128]{1,0:T(8,128)(2,1)S(1)} %get-tuple-element.28), channel_id=1, source_target_pairs={{0,192},{64,128},{128,64},{192,0},{256,448},{320,384},{384,320},{4... | collective-permute-start | bytes 208904 | tf_op jit(solution)/shard_map/ppermute | solution.py:197
  119.8 0.0 all-to-all-done.in_ref
  119.8 0.9 lay.1.refs_4_
  120.7 0.0 collective-permute-done.5.refs_1_
  120.7 0.0 collective-permute-done.6.refs_2_
  120.7 1.4 %collective-permute-done.7.refs_3_ = bf16[272,128]{1,0:T(8,128)(2,1)S(1)} collective-permute-done((bf16[272,128]{1,0:T(8,128)(2,1)S(1)}, bf16[272,128]{1,0:T(8,128)(2,1)S(1)}, u32[]{:S(2)}, u32[]{:S(2)}) %collective-permute-start.7) | collective-permute-done | bytes 69664 | tf_op jit(solution)/shard_map/ppermute | solution.py:197
  122.0 1.6 %finish.1 = (bf16[4,1536]{1,0:T(4,128)(2,1)}, bf16[64,8192]{1,0:T(8,128)(2,1)}) custom-call(bf16[272,128]{1,0:T(8,128)(2,1)S(1)} %get-tuple-element.25.refs_0_, bf16[272,128]{1,0:T(8,128)(2,1)S(1)} %collective-permute-done.5.refs_1_, bf16[272,128]{1,0:T(8,128)(2,1)S(1)} %collective-permute-done.6.refs_2_, ...), custom_call_target="tpu_custom_call", output_to_operand_aliasing={{1}: (4, {})} | custom-call | tf_op jit(solution)/shard_map/finish/pallas_call | solution.py:301
  (2 shorter events, 0.0 us)
Async XLA Ops:
  7.2 112.5 %all-to-all-start = ((bf16[64,56,128]{2,1,0:T(8,128)(2,1)}), bf16[64,56,128]{2,1,0:T(8,128)(2,1)S(1)}, u32[]{:S(2)}, u32[]{:S(2)}) async-start(bf16[64,56,128]{2,1,0:T(8,128)(2,1)} %bitcast.5), calls=%async_computation | async-start | bytes 1835008 | tf_op jit(solution)/shard_map/all_to_all | solution.py:354
  29.2 52.1 %collective-permute-start = (bf16[328,128]{1,0:T(8,128)(2,1)}, bf16[328,128]{1,0:T(8,128)(2,1)S(1)}, u32[]{:S(2)}, u32[]{:S(2)}) collective-permute-start(bf16[328,128]{1,0:T(8,128)(2,1)} %get-tuple-element.18), channel_id=1, source_target_pairs={{0,256},{64,320},{128,384},{192,448},{256,0},{320,64},{384,128},{4... | collective-permute-start | bytes 251912 | tf_op jit(solution)/shard_map/ppermute | solution.py:197
  81.3 0.9 copy-start
  82.2 10.1 %collective-permute-start.1 = (bf16[272,128]{1,0:T(8,128)(2,1)S(1)}, bf16[272,128]{1,0:T(8,128)(2,1)S(1)}, u32[]{:S(2)}, u32[]{:S(2)}) collective-permute-start(bf16[272,128]{1,0:T(8,128)(2,1)S(1)} %get-tuple-element.20), channel_id=1, source_target_pairs={{0,8},{8,0},{16,24},{24,16},{32,40},{40,32},{48,56},{56,48},{1,9},... | collective-permute-start | bytes 208904 | tf_op jit(solution)/shard_map/ppermute | solution.py:197
  85.6 8.5 %collective-permute-start.2 = (bf16[272,128]{1,0:T(8,128)(2,1)S(1)}, bf16[272,128]{1,0:T(8,128)(2,1)S(1)}, u32[]{:S(2)}, u32[]{:S(2)}) collective-permute-start(bf16[272,128]{1,0:T(8,128)(2,1)S(1)} %get-tuple-element.21), channel_id=1, source_target_pairs={{0,16},{8,24},{16,0},{24,8},{32,48},{40,56},{48,32},{56,40},{1,17}... | collective-permute-start | bytes 208904 | tf_op jit(solution)/shard_map/ppermute | solution.py:197
  89.9 8.0 %collective-permute-start.3 = (bf16[272,128]{1,0:T(8,128)(2,1)S(1)}, bf16[272,128]{1,0:T(8,128)(2,1)S(1)}, u32[]{:S(2)}, u32[]{:S(2)}) collective-permute-start(bf16[272,128]{1,0:T(8,128)(2,1)S(1)} %get-tuple-element.22), channel_id=1, source_target_pairs={{0,24},{8,16},{16,8},{24,0},{32,56},{40,48},{48,40},{56,32},{1,25}... | collective-permute-start | bytes 208904 | tf_op jit(solution)/shard_map/ppermute | solution.py:197
  98.0 11.6 %collective-permute-start.4 = (bf16[400,128]{1,0:T(8,128)(2,1)S(1)}, bf16[400,128]{1,0:T(8,128)(2,1)S(1)}, u32[]{:S(2)}, u32[]{:S(2)}) collective-permute-start(bf16[400,128]{1,0:T(8,128)(2,1)S(1)} %get-tuple-element.24), channel_id=1, source_target_pairs={{0,32},{8,40},{16,48},{24,56},{32,0},{40,8},{48,16},{56,24},{1,33}... | collective-permute-start | bytes 307208 | tf_op jit(solution)/shard_map/ppermute | solution.py:197
  109.6 11.0 %collective-permute-start.5 = (bf16[272,128]{1,0:T(8,128)(2,1)S(1)}, bf16[272,128]{1,0:T(8,128)(2,1)S(1)}, u32[]{:S(2)}, u32[]{:S(2)}) collective-permute-start(bf16[272,128]{1,0:T(8,128)(2,1)S(1)} %get-tuple-element.26), channel_id=1, source_target_pairs={{0,64},{64,0},{128,192},{192,128},{256,320},{320,256},{384,448},{4... | collective-permute-start | bytes 208904 | tf_op jit(solution)/shard_map/ppermute | solution.py:197
  111.5 9.1 %collective-permute-start.6 = (bf16[272,128]{1,0:T(8,128)(2,1)S(1)}, bf16[272,128]{1,0:T(8,128)(2,1)S(1)}, u32[]{:S(2)}, u32[]{:S(2)}) collective-permute-start(bf16[272,128]{1,0:T(8,128)(2,1)S(1)} %get-tuple-element.27), channel_id=1, source_target_pairs={{0,128},{64,192},{128,0},{192,64},{256,384},{320,448},{384,256},{4... | collective-permute-start | bytes 208904 | tf_op jit(solution)/shard_map/ppermute | solution.py:197
  113.5 8.6 %collective-permute-start.7 = (bf16[272,128]{1,0:T(8,128)(2,1)S(1)}, bf16[272,128]{1,0:T(8,128)(2,1)S(1)}, u32[]{:S(2)}, u32[]{:S(2)}) collective-permute-start(bf16[272,128]{1,0:T(8,128)(2,1)S(1)} %get-tuple-element.28), channel_id=1, source_target_pairs={{0,192},{64,128},{128,64},{192,0},{256,448},{320,384},{384,320},{4... | collective-permute-start | bytes 208904 | tf_op jit(solution)/shard_map/ppermute | solution.py:197

commit v4 on v3

--- a/solution.py
+++ b/solution.py
@@ -51,7 +51,8 @@
     row = lax.broadcasted_iota(jnp.int32, (SLOT, LANES), 0)
     offset = jnp.zeros((SLOT, LANES), F32)
     for h in range(heads):
-        rows[pl.ds(h, seqs, stride=SLOT), :HD] = query_ref[:, h * HD : (h + 1) * HD].astype(F32)
+        query = query_ref[:, h * HD : (h + 1) * HD].astype(F32)
+        rows[pl.ds(h, seqs, stride=SLOT), :] = jnp.concatenate([query, query], axis=1)
         offset = jnp.where(row == h, offset_ref[h], offset)
     return offset
 
@@ -69,13 +70,15 @@
     seqs = kv.shape[0]
     slots = seqs * SLOT
     row_head = lax.broadcasted_iota(jnp.int32, (SLOT, LANES), 0) // group
+    odd = lax.broadcasted_iota(jnp.int32, (SLOT, LANES), 1) // HD
     logits = []
     for s in range(seqs):
-        queries = rows[s * SLOT : (s + 1) * SLOT, :HD].astype(BF16)
-        total = jnp.zeros((SLOT, LANES), F32)
-        for n in range(KVH):
-            part = jnp.dot(queries, kv[s, n], preferred_element_type=F32)
-            total = jnp.where(row_head == n, part, total)
+        queries = rows[s * SLOT : (s + 1) * SLOT]
+        own = [jnp.where(row_head == n + odd, queries, 0.0) for n in range(0, KVH, 2)]
+        keys = kv[s, :KVH].reshape(KVH * HD, LANES)
+        total = jnp.dot(
+            jnp.concatenate(own, axis=1).astype(BF16), keys, preferred_element_type=F32
+        )
         logits.append(total * HD ** (-0.5) + offset)
     logit = jnp.concatenate(logits, axis=0)
     soft = jnp.log1p(jnp.exp(-jnp.abs(logit)))

time: 124 us -> 124 us (level)
  no operation moved by 1% of the time
where the time goes in v4:
time: 124 us
  waiting for transfers between devices  58.3 us (47%)
  starting transfers between devices  54.4 us (44%)
  Pallas kernels  9.28 us (7%)
    ppermute x8, waiting for transfers between devices, partner(): lax.ppermute(block, axis, [(i, i ^ distance) for i in range(lax.axis_size...  58.3 us
    ppermute x8, starting transfers between devices, partner(): lax.ppermute(block, axis, [(i, i ^ distance) for i in range(lax.axis_size...  32.4 us
    all_to_all x1, starting transfers between devices, local(): lax.all_to_all(projected.reshape(slots, width - SIDE, positions), SP, spl...  22 us
    pallas_call x1, Pallas kernels, project(): pl.pallas_call(project_kernel, in_specs=[pl.BlockSpec(memory_space=pltpu....  6.61 us
  transfers between devices with their start and end apart: 9, of which 5 were waited for; matrix products, arithmetic and copies ran while one was open for 0% of the time, Pallas kernels for 1%

profile of v4, /device:TPU:6, one launch (start us, length us, event | category | flops | bytes accessed | tf_op | source)
XLA Modules:
  0.0 123.6 jit_solution(8329909122407116629)
XLA Ops:
  0.6 6.6 %project.1 = (bf16[4,16,56,128]{3,2,1,0:T(8,128)(2,1)}, bf16[328,128]{1,0:T(8,128)(2,1)}, bf16[328,128]{1,0:T(8,128)(2,1)}) custom-call(bf16[4,128,2048]{2,1,0:T(8,128)(2,1)} %x_hbm.1, bf16[2048,1024]{1,0:T(8,128)(2,1)} %w_hbm.1, bf16[4,1536]{1,0:T(4,128)(2,1)} %query_ref.1, f32[24]{0:T(128)} %offset_ref.1), custom_call_target="tpu_custom_call" | custom-call | tf_op jit(solution)/shard_map/project/pallas_call | solution.py:172
  7.2 22.0 %all-to-all-start = ((bf16[64,56,128]{2,1,0:T(8,128)(2,1)}), bf16[64,56,128]{2,1,0:T(8,128)(2,1)S(1)}, u32[]{:S(2)}, u32[]{:S(2)}) async-start(bf16[64,56,128]{2,1,0:T(8,128)(2,1)} %bitcast.5), calls=%async_computation | async-start | bytes 1835008 | tf_op jit(solution)/shard_map/all_to_all | solution.py:357
  29.2 7.5 %collective-permute-start = (bf16[328,128]{1,0:T(8,128)(2,1)}, bf16[328,128]{1,0:T(8,128)(2,1)S(1)}, u32[]{:S(2)}, u32[]{:S(2)}) collective-permute-start(bf16[328,128]{1,0:T(8,128)(2,1)} %get-tuple-element.18), channel_id=1, source_target_pairs={{0,256},{64,320},{128,384},{192,448},{256,0},{320,64},{384,128},{4... | collective-permute-start | bytes 251912 | tf_op jit(solution)/shard_map/ppermute | solution.py:200
  36.7 44.6 %collective-permute-done.refs_1_ = bf16[328,128]{1,0:T(8,128)(2,1)S(1)} collective-permute-done((bf16[328,128]{1,0:T(8,128)(2,1)}, bf16[328,128]{1,0:T(8,128)(2,1)S(1)}, u32[]{:S(2)}, u32[]{:S(2)}) %collective-permute-start) | collective-permute-done | bytes 84000 | tf_op jit(solution)/shard_map/ppermute | solution.py:200
  81.3 0.9 copy-done
  82.2 3.4 %collective-permute-start.1 = (bf16[272,128]{1,0:T(8,128)(2,1)S(1)}, bf16[272,128]{1,0:T(8,128)(2,1)S(1)}, u32[]{:S(2)}, u32[]{:S(2)}) collective-permute-start(bf16[272,128]{1,0:T(8,128)(2,1)S(1)} %get-tuple-element.20), channel_id=1, source_target_pairs={{0,8},{8,0},{16,24},{24,16},{32,40},{40,32},{48,56},{56,48},{1,9},... | collective-permute-start | bytes 208904 | tf_op jit(solution)/shard_map/ppermute | solution.py:200
  85.6 4.3 %collective-permute-start.2 = (bf16[272,128]{1,0:T(8,128)(2,1)S(1)}, bf16[272,128]{1,0:T(8,128)(2,1)S(1)}, u32[]{:S(2)}, u32[]{:S(2)}) collective-permute-start(bf16[272,128]{1,0:T(8,128)(2,1)S(1)} %get-tuple-element.21), channel_id=1, source_target_pairs={{0,16},{8,24},{16,0},{24,8},{32,48},{40,56},{48,32},{56,40},{1,17}... | collective-permute-start | bytes 208904 | tf_op jit(solution)/shard_map/ppermute | solution.py:200
  89.9 2.5 %collective-permute-start.3 = (bf16[272,128]{1,0:T(8,128)(2,1)S(1)}, bf16[272,128]{1,0:T(8,128)(2,1)S(1)}, u32[]{:S(2)}, u32[]{:S(2)}) collective-permute-start(bf16[272,128]{1,0:T(8,128)(2,1)S(1)} %get-tuple-element.22), channel_id=1, source_target_pairs={{0,24},{8,16},{16,8},{24,0},{32,56},{40,48},{48,40},{56,32},{1,25}... | collective-permute-start | bytes 208904 | tf_op jit(solution)/shard_map/ppermute | solution.py:200
  92.4 0.0 collective-permute-done.1.refs_1_
  92.4 1.7 %collective-permute-done.2.refs_2_ = bf16[272,128]{1,0:T(8,128)(2,1)S(1)} collective-permute-done((bf16[272,128]{1,0:T(8,128)(2,1)S(1)}, bf16[272,128]{1,0:T(8,128)(2,1)S(1)}, u32[]{:S(2)}, u32[]{:S(2)}) %collective-permute-start.2) | collective-permute-done | bytes 69664 | tf_op jit(solution)/shard_map/ppermute | solution.py:200
  94.1 3.8 %collective-permute-done.3.refs_3_ = bf16[272,128]{1,0:T(8,128)(2,1)S(1)} collective-permute-done((bf16[272,128]{1,0:T(8,128)(2,1)S(1)}, bf16[272,128]{1,0:T(8,128)(2,1)S(1)}, u32[]{:S(2)}, u32[]{:S(2)}) %collective-permute-start.3) | collective-permute-done | bytes 69664 | tf_op jit(solution)/shard_map/ppermute | solution.py:200
  97.9 0.1 shard_map.60
  98.0 4.7 %collective-permute-start.4 = (bf16[400,128]{1,0:T(8,128)(2,1)S(1)}, bf16[400,128]{1,0:T(8,128)(2,1)S(1)}, u32[]{:S(2)}, u32[]{:S(2)}) collective-permute-start(bf16[400,128]{1,0:T(8,128)(2,1)S(1)} %get-tuple-element.24), channel_id=1, source_target_pairs={{0,32},{8,40},{16,48},{24,56},{32,0},{40,8},{48,16},{56,24},{1,33}... | collective-permute-start | bytes 307208 | tf_op jit(solution)/shard_map/ppermute | solution.py:200
  102.7 6.9 %collective-permute-done.4.refs_1_ = bf16[400,128]{1,0:T(8,128)(2,1)S(1)} collective-permute-done((bf16[400,128]{1,0:T(8,128)(2,1)S(1)}, bf16[400,128]{1,0:T(8,128)(2,1)S(1)}, u32[]{:S(2)}, u32[]{:S(2)}) %collective-permute-start.4) | collective-permute-done | bytes 102432 | tf_op jit(solution)/shard_map/ppermute | solution.py:200
  109.6 0.1 shard_map.61
  109.6 1.9 %collective-permute-start.5 = (bf16[272,128]{1,0:T(8,128)(2,1)S(1)}, bf16[272,128]{1,0:T(8,128)(2,1)S(1)}, u32[]{:S(2)}, u32[]{:S(2)}) collective-permute-start(bf16[272,128]{1,0:T(8,128)(2,1)S(1)} %get-tuple-element.26), channel_id=1, source_target_pairs={{0,64},{64,0},{128,192},{192,128},{256,320},{320,256},{384,448},{4... | collective-permute-start | bytes 208904 | tf_op jit(solution)/shard_map/ppermute | solution.py:200
  111.6 1.9 %collective-permute-start.6 = (bf16[272,128]{1,0:T(8,128)(2,1)S(1)}, bf16[272,128]{1,0:T(8,128)(2,1)S(1)}, u32[]{:S(2)}, u32[]{:S(2)}) collective-permute-start(bf16[272,128]{1,0:T(8,128)(2,1)S(1)} %get-tuple-element.27), channel_id=1, source_target_pairs={{0,128},{64,192},{128,0},{192,64},{256,384},{320,448},{384,256},{4... | collective-permute-start | bytes 208904 | tf_op jit(solution)/shard_map/ppermute | solution.py:200
  113.5 6.3 %collective-permute-start.7 = (bf16[272,128]{1,0:T(8,128)(2,1)S(1)}, bf16[272,128]{1,0:T(8,128)(2,1)S(1)}, u32[]{:S(2)}, u32[]{:S(2)}) collective-permute-start(bf16[272,128]{1,0:T(8,128)(2,1)S(1)} %get-tuple-element.28), channel_id=1, source_target_pairs={{0,192},{64,128},{128,64},{192,0},{256,448},{320,384},{384,320},{4... | collective-permute-start | bytes 208904 | tf_op jit(solution)/shard_map/ppermute | solution.py:200
  119.8 0.0 all-to-all-done.in_ref
  119.8 0.9 lay.1.refs_4_
  120.7 0.0 collective-permute-done.5.refs_1_
  120.7 0.0 collective-permute-done.6.refs_2_
  120.7 1.4 %collective-permute-done.7.refs_3_ = bf16[272,128]{1,0:T(8,128)(2,1)S(1)} collective-permute-done((bf16[272,128]{1,0:T(8,128)(2,1)S(1)}, bf16[272,128]{1,0:T(8,128)(2,1)S(1)}, u32[]{:S(2)}, u32[]{:S(2)}) %collective-permute-start.7) | collective-permute-done | bytes 69664 | tf_op jit(solution)/shard_map/ppermute | solution.py:200
  122.0 1.6 %finish.1 = (bf16[4,1536]{1,0:T(4,128)(2,1)}, bf16[64,8192]{1,0:T(8,128)(2,1)}) custom-call(bf16[272,128]{1,0:T(8,128)(2,1)S(1)} %get-tuple-element.25.refs_0_, bf16[272,128]{1,0:T(8,128)(2,1)S(1)} %collective-permute-done.5.refs_1_, bf16[272,128]{1,0:T(8,128)(2,1)S(1)} %collective-permute-done.6.refs_2_, ...), custom_call_target="tpu_custom_call", output_to_operand_aliasing={{1}: (4, {})} | custom-call | tf_op jit(solution)/shard_map/finish/pallas_call | solution.py:304
  (2 shorter events, 0.0 us)
Async XLA Ops:
  7.2 112.5 %all-to-all-start = ((bf16[64,56,128]{2,1,0:T(8,128)(2,1)}), bf16[64,56,128]{2,1,0:T(8,128)(2,1)S(1)}, u32[]{:S(2)}, u32[]{:S(2)}) async-start(bf16[64,56,128]{2,1,0:T(8,128)(2,1)} %bitcast.5), calls=%async_computation | async-start | bytes 1835008 | tf_op jit(solution)/shard_map/all_to_all | solution.py:357
  29.2 52.1 %collective-permute-start = (bf16[328,128]{1,0:T(8,128)(2,1)}, bf16[328,128]{1,0:T(8,128)(2,1)S(1)}, u32[]{:S(2)}, u32[]{:S(2)}) collective-permute-start(bf16[328,128]{1,0:T(8,128)(2,1)} %get-tuple-element.18), channel_id=1, source_target_pairs={{0,256},{64,320},{128,384},{192,448},{256,0},{320,64},{384,128},{4... | collective-permute-start | bytes 251912 | tf_op jit(solution)/shard_map/ppermute | solution.py:200
  81.3 0.9 copy-start
  82.2 10.1 %collective-permute-start.1 = (bf16[272,128]{1,0:T(8,128)(2,1)S(1)}, bf16[272,128]{1,0:T(8,128)(2,1)S(1)}, u32[]{:S(2)}, u32[]{:S(2)}) collective-permute-start(bf16[272,128]{1,0:T(8,128)(2,1)S(1)} %get-tuple-element.20), channel_id=1, source_target_pairs={{0,8},{8,0},{16,24},{24,16},{32,40},{40,32},{48,56},{56,48},{1,9},... | collective-permute-start | bytes 208904 | tf_op jit(solution)/shard_map/ppermute | solution.py:200
  85.6 8.5 %collective-permute-start.2 = (bf16[272,128]{1,0:T(8,128)(2,1)S(1)}, bf16[272,128]{1,0:T(8,128)(2,1)S(1)}, u32[]{:S(2)}, u32[]{:S(2)}) collective-permute-start(bf16[272,128]{1,0:T(8,128)(2,1)S(1)} %get-tuple-element.21), channel_id=1, source_target_pairs={{0,16},{8,24},{16,0},{24,8},{32,48},{40,56},{48,32},{56,40},{1,17}... | collective-permute-start | bytes 208904 | tf_op jit(solution)/shard_map/ppermute | solution.py:200
  89.9 8.0 %collective-permute-start.3 = (bf16[272,128]{1,0:T(8,128)(2,1)S(1)}, bf16[272,128]{1,0:T(8,128)(2,1)S(1)}, u32[]{:S(2)}, u32[]{:S(2)}) collective-permute-start(bf16[272,128]{1,0:T(8,128)(2,1)S(1)} %get-tuple-element.22), channel_id=1, source_target_pairs={{0,24},{8,16},{16,8},{24,0},{32,56},{40,48},{48,40},{56,32},{1,25}... | collective-permute-start | bytes 208904 | tf_op jit(solution)/shard_map/ppermute | solution.py:200
  98.0 11.6 %collective-permute-start.4 = (bf16[400,128]{1,0:T(8,128)(2,1)S(1)}, bf16[400,128]{1,0:T(8,128)(2,1)S(1)}, u32[]{:S(2)}, u32[]{:S(2)}) collective-permute-start(bf16[400,128]{1,0:T(8,128)(2,1)S(1)} %get-tuple-element.24), channel_id=1, source_target_pairs={{0,32},{8,40},{16,48},{24,56},{32,0},{40,8},{48,16},{56,24},{1,33}... | collective-permute-start | bytes 307208 | tf_op jit(solution)/shard_map/ppermute | solution.py:200
  109.6 11.0 %collective-permute-start.5 = (bf16[272,128]{1,0:T(8,128)(2,1)S(1)}, bf16[272,128]{1,0:T(8,128)(2,1)S(1)}, u32[]{:S(2)}, u32[]{:S(2)}) collective-permute-start(bf16[272,128]{1,0:T(8,128)(2,1)S(1)} %get-tuple-element.26), channel_id=1, source_target_pairs={{0,64},{64,0},{128,192},{192,128},{256,320},{320,256},{384,448},{4... | collective-permute-start | bytes 208904 | tf_op jit(solution)/shard_map/ppermute | solution.py:200
  111.6 9.1 %collective-permute-start.6 = (bf16[272,128]{1,0:T(8,128)(2,1)S(1)}, bf16[272,128]{1,0:T(8,128)(2,1)S(1)}, u32[]{:S(2)}, u32[]{:S(2)}) collective-permute-start(bf16[272,128]{1,0:T(8,128)(2,1)S(1)} %get-tuple-element.27), channel_id=1, source_target_pairs={{0,128},{64,192},{128,0},{192,64},{256,384},{320,448},{384,256},{4... | collective-permute-start | bytes 208904 | tf_op jit(solution)/shard_map/ppermute | solution.py:200
  113.5 8.6 %collective-permute-start.7 = (bf16[272,128]{1,0:T(8,128)(2,1)S(1)}, bf16[272,128]{1,0:T(8,128)(2,1)S(1)}, u32[]{:S(2)}, u32[]{:S(2)}) collective-permute-start(bf16[272,128]{1,0:T(8,128)(2,1)S(1)} %get-tuple-element.28), channel_id=1, source_target_pairs={{0,192},{64,128},{128,64},{192,0},{256,448},{320,384},{384,320},{4... | collective-permute-start | bytes 208904 | tf_op jit(solution)/shard_map/ppermute | solution.py:200
